TPU v7x, 128 devices: a whole 4x4x4 slice. The times are simulated.
128 devices in a mesh: ep: 128 (over z, y, x, core).
Axes of the slice: x: 4, y: 4, z: 4, core: 2. Of those that a mesh axis runs over, the one named last changes fastest.
Arguments:
- tokens: bfloat16 [2048, 2048], P('ep'), may hold values from -6 to 6
- recurrent_state: float32 [2048, 16, 4096], P('ep'), may hold values from -8 to 8
- first_gain: float32 [2048], replicated, may hold values from 0.1 to 1.9
- w_receptance: bfloat16 [2048, 1024], P('ep'), may hold values from -0.125 to 0.125
- w_key: bfloat16 [2048, 1024], P('ep'), may hold values from -0.125 to 0.125
- w_value: bfloat16 [2048, 1024], P('ep'), may hold values from -0.125 to 0.125
- decay_down: bfloat16 [2048, 64], replicated, may hold values from -0.125 to 0.125
- decay_up: bfloat16 [64, 1024], replicated, may hold values from -0.75 to 0.75
- decay_base: float32 [1024], replicated, may hold values from -4 to 1
- rate_down: bfloat16 [2048, 64], replicated, may hold values from -0.125 to 0.125
- rate_up: bfloat16 [64, 1024], replicated, may hold values from -0.75 to 0.75
- rate_base: float32 [1024], replicated, may hold values from -5 to 5
- key_scale: float32 [1024], replicated, may hold values from 0.25 to 4
- head_gain: float32 [1024], replicated, may hold values from 0.1 to 1.9
- w_output: bfloat16 [1024, 2048], replicated, may hold values from -0.1875 to 0.1875
- second_gain: float32 [2048], replicated, may hold values from 0.1 to 1.9
- shared_gate: bfloat16 [2048, 512], replicated, may hold values from -0.125 to 0.125
- shared_up: bfloat16 [2048, 512], replicated, may hold values from -0.125 to 0.125
- shared_down: bfloat16 [512, 2048], replicated, may hold values from -0.25 to 0.25
- expert_gate: bfloat16 [128, 2048, 512], P('ep'), may hold values from -0.125 to 0.125
- expert_up: bfloat16 [128, 2048, 512], P('ep'), may hold values from -0.125 to 0.125
- expert_down: bfloat16 [128, 512, 2048], P('ep'), may hold values from -0.25 to 0.25
- routes: int32 [2048, 4], replicated, may hold values from 0 to 127, all different within a row; in each aligned block of 16 rows (0 to 15, 16 to 31, ...) at most 4 rows name the same one
- route_weights: float32 [2048, 4], replicated, may hold values from 0.1 to 1
Outputs:
- new_tokens: bfloat16 [2048, 2048], P('ep')
- new_state: float32 [2048, 16, 4096], P('ep')
Inputs may be any that keep to these rules, and one draw needn't show every extreme that they name: `routes`: each row names 4 different experts. In the rows of one device no expert is named by more than 4 rows, a bound that some block reaches of them.
All inputs are finite; a program needn't handle non-finite values.
Results may differ from a plain program's by a relative error of at most 0.015.
Values may be sent and summed in bfloat16 or wider, within the bound.
A program may use at most 128 MiB of HBM per device.

v0:
```python
import functools

import jax
import jax.numpy as jnp
from jax import lax
from jax.experimental import pallas as pl
from jax.experimental.pallas import tpu as pltpu
from jax.sharding import PartitionSpec as P

HEAD = 64
TOPK = 4
MOST = 4
GROUP = 8
PARTS = 4
NORM_EPS = 1e-06
GROUP_EPS = 0.00064
MESH = pl.DeviceIdType.MESH
F32 = jnp.float32
BF16 = jnp.bfloat16
VMEM_BYTES = 60 * 1024 * 1024


def dot(a, b):
    return jnp.dot(a, b, preferred_element_type=F32)


def rms_scale(inputs, gain):
    widened = inputs.astype(F32)
    return (
        widened * lax.rsqrt(jnp.mean(widened * widened, axis=-1, keepdims=True) + NORM_EPS) * gain
    )


def project_kernel(
    devices,
    tokens,
    gain,
    w_r,
    w_k,
    w_v,
    decay_down,
    decay_up,
    decay_base,
    rate_down,
    rate_up,
    rate_base,
    key_scale,
    out,
    stage,
    wbuf,
    nsend,
    xbuf,
    psend,
    precv,
    local_sem,
    wsend_sem,
    wrecv_sem,
    xsend_sem,
    xrecv_sem,
    psend_sem,
    precv_sem,
):
    rows, mix = w_r.shape
    half = mix // 2
    count = tokens.shape[0]
    groups = devices // GROUP
    members = 2 * groups
    depth = tokens.shape[1] // groups
    me = lax.axis_index("ep")
    base = (me // GROUP) * GROUP
    place = me % GROUP
    core = me % 2
    column = place // 2
    member = (me // GROUP) * 2 + core
    chip = me - core
    x_bit = (place // 2) % 2
    y_bit = place // 4
    x_chip = chip + 2 - 4 * x_bit
    y_chip = chip + 4 - 8 * y_bit
    diag_chip = x_chip + 4 - 8 * y_bit
    partner = chip + 1 - core

    def peer_of(offset):
        which = (member + offset) % members
        return which, (which // 2) * GROUP + column * 2 + which % 2

    local = []
    weights = (w_r, w_k, w_v)
    for number, weight in enumerate(weights):
        for side in range(2):
            local.append(
                pltpu.make_async_copy(
                    weight.at[:, pl.ds(side * half, half)],
                    stage.at[number, side],
                    local_sem.at[number * 2 + side],
                )
            )
    for copy in local:
        copy.start()

    barrier = pltpu.get_barrier_semaphore()
    greet = [partner, x_chip, x_chip + 1, y_chip, y_chip + 1]
    greet = greet + [peer_of(offset)[1] for offset in range(1, members)]
    for peer in greet:
        pl.semaphore_signal(barrier, inc=1, device_id=(peer,), device_id_type=MESH)

    normed = rms_scale(tokens[...], gain[...]).astype(BF16)
    for number in range(groups):
        nsend[number] = normed[:, number * depth : (number + 1) * depth]
    for copy in local:
        copy.wait()
    pl.semaphore_wait(barrier, len(greet))

    def slot(number, device):
        return wbuf.at[number, pl.ds(pl.multiple_of((device - base) * rows, rows), rows), :]

    def weight_copy(number, source, landing, send, receive, target):
        return pltpu.make_async_remote_copy(
            src_ref=source,
            dst_ref=slot(number, landing),
            send_sem=wsend_sem.at[number * 7 + send],
            recv_sem=wrecv_sem.at[number * 7 + receive],
            device_id=(target,),
            device_id_type=MESH,
        )

    sends = []

    def launch(copy):
        copy.start()
        sends.append(copy)

    def direct(number):
        for side in range(2):
            source = stage.at[number, side]
            launch(weight_copy(number, source, me, 1 + side, 1 + core, x_chip + side))
            launch(weight_copy(number, source, me, 3 + side, 3 + core, y_chip + side))
        launch(weight_copy(number, stage.at[number, 1 - core], me, 0, 0, partner))

    def arrived(number, source, receive):
        weight_copy(number, stage.at[0, 0], source, 0, receive, partner).wait_recv()

    def relay(number):
        arrived(number, y_chip, 3)
        launch(weight_copy(number, slot(number, y_chip), y_chip, 5, 5, x_chip + core))
        arrived(number, x_chip + 1, 2)
        launch(weight_copy(number, slot(number, x_chip + 1), x_chip + 1, 6, 6, y_chip + core))

    direct(0)
    for offset in range(1, members):
        which, device = peer_of(offset)
        launch(
            pltpu.make_async_remote_copy(
                src_ref=nsend.at[which // 2],
                dst_ref=xbuf.at[member],
                send_sem=xsend_sem.at[offset],
                recv_sem=xrecv_sem.at[offset],
                device_id=(device,),
                device_id_type=MESH,
            )
        )
    direct(1)

    for number in range(3):
        own = stage[number, core]
        wbuf[number, pl.ds(pl.multiple_of(place * rows, rows), rows), :] = own
    xbuf[member] = nsend[me // GROUP]
    relay(0)
    direct(2)

    def put(number, values, first):
        for head in range(values.shape[1] // HEAD):
            out[number, :, first + head, :] = values[:, head * HEAD : (head + 1) * HEAD]

    heads = mix // HEAD
    flip = (((1,), (1,)), ((), ()))

    def down(matrix):
        return lax.dot_general(normed, matrix, flip, preferred_element_type=F32)

    decay_low = jnp.tanh(down(decay_down[...])).astype(BF16)
    decay_pre = decay_base[...] + dot(decay_low, decay_up[...])
    put(3, jnp.exp(-jnp.exp(-jax.nn.softplus(-decay_pre) - 0.5)), 0)
    rate_low = down(rate_down[...]).astype(BF16)
    put(4, jax.nn.sigmoid(rate_base[...] + dot(rate_low, rate_up[...])), 0)

    for offset in range(1, members):
        source = (member + members - offset) % members
        pltpu.make_async_remote_copy(
            src_ref=nsend.at[0],
            dst_ref=xbuf.at[source],
            send_sem=xsend_sem.at[offset],
            recv_sem=xrecv_sem.at[offset],
            device_id=(partner,),
            device_id_type=MESH,
        ).wait_recv()
    stacked = xbuf[...].reshape(members * count, depth)

    def part_copy(number, source, landing, offset, target):
        return pltpu.make_async_remote_copy(
            src_ref=psend.at[number, source],
            dst_ref=precv.at[number, landing],
            send_sem=psend_sem.at[number * members + offset],
            recv_sem=precv_sem.at[number * members + offset],
            device_id=(target,),
            device_id_type=MESH,
        )

    def multiply(number):
        arrived(number, partner, 0)
        arrived(number, x_chip, 1)
        arrived(number, y_chip + 1, 4)
        arrived(number, diag_chip, 5)
        arrived(number, diag_chip + 1, 6)
        part = dot(stacked, wbuf[number]).astype(BF16)
        psend[number] = part.reshape(members, count, half)
        for offset in range(1, members):
            which, device = peer_of(offset)
            launch(part_copy(number, which, member, offset, device))
        precv[number, member] = psend[number, member]

    def finish(number):
        for offset in range(1, members):
            source = (member + members - offset) % members
            part_copy(number, 0, source, offset, partner).wait_recv()
        for side in range(2):
            total = precv[number, side].astype(F32)
            for which in range(1, groups):
                total = total + precv[number, which * 2 + side].astype(F32)
            total = total.astype(BF16).astype(F32)
            put(number, total, side * (heads // 2))
            if number == 1:
                scale = key_scale[:, side * half : (side + 1) * half]
                put(5, total * scale, side * (heads // 2))

    relay(1)
    multiply(0)
    relay(2)
    multiply(1)
    finish(0)
    multiply(2)
    finish(1)
    finish(2)
    for copy in sends:
        copy.wait_send()


def project(devices, tokens, gain, w_r, w_k, w_v, dd, du, db, rd, ru, rb, scale):
    count, width = tokens.shape
    rows, mix = w_r.shape
    groups = devices // GROUP
    members = 2 * groups
    half = mix // 2
    vmem = pl.BlockSpec(memory_space=pltpu.VMEM)
    hbm = pl.BlockSpec(memory_space=pl.ANY)
    dma = pltpu.SemaphoreType.DMA
    return pl.pallas_call(
        functools.partial(project_kernel, devices),
        out_shape=jax.ShapeDtypeStruct((6, count, mix // HEAD, HEAD), F32),
        in_specs=[vmem, vmem, hbm, hbm, hbm] + [vmem] * 7,
        out_specs=vmem,
        scratch_shapes=[
            pltpu.VMEM((3, 2, rows, half), BF16),
            pltpu.VMEM((3, GROUP * rows, half), BF16),
            pltpu.VMEM((groups, count, width // groups), BF16),
            pltpu.VMEM((members, count, width // groups), BF16),
            pltpu.VMEM((3, members, count, half), BF16),
            pltpu.VMEM((3, members, count, half), BF16),
            dma((6,)),
            dma((21,)),
            dma((21,)),
            dma((members,)),
            dma((members,)),
            dma((3 * members,)),
            dma((3 * members,)),
        ],
        compiler_params=pltpu.CompilerParams(
            collective_id=0, has_side_effects=True, vmem_limit_bytes=VMEM_BYTES
        ),
        name="project",
    )(tokens, gain, w_r, w_k, w_v, dd, du, db, rd, ru, rb, scale)


def split_sum(values, ones):
    high = values.astype(BF16)
    low = (values - high.astype(F32)).astype(BF16)
    return dot(high, ones) + dot(low, ones)


def mixer_kernel(
    steps,
    vectors,
    state,
    head_gain,
    tokens,
    w_output,
    second_gain,
    new_state,
    residual,
    second,
    wbuf,
    mixed,
    sem,
):
    step = pl.program_id(0)
    _, per_step, heads, _ = vectors.shape
    entries = state.shape[2]
    span = 256
    tiles = entries // span
    copies = span // HEAD
    copy = pltpu.make_async_copy(w_output, wbuf, sem)

    @pl.when(step == 0)
    def _():
        copy.start()

    row = lax.broadcasted_iota(jnp.int32, (span, span), 0)
    col = lax.broadcasted_iota(jnp.int32, (span, span), 1)
    ones = (row // HEAD == col // HEAD).astype(F32).astype(BF16)
    lane = lax.broadcasted_iota(jnp.int32, (heads, span), 1)

    def widen(inputs):
        return jnp.concatenate([inputs] * copies, axis=1)

    for number in range(per_step):
        reader, keys, values, decay, learn, scaled = [vectors[w, number] for w in range(6)]
        direction = scaled / jnp.sqrt(jnp.sum(scaled * scaled, axis=-1, keepdims=True) + 1.0)
        wide_direction = widen(direction)
        wide_decay = widen(decay)
        wide_learn = widen(direction * learn)
        wide_keys = widen(keys)
        wide_reader = widen(reader)
        wide_values = widen(values)
        blocks = [state[number, :, i * span : (i + 1) * span] for i in range(tiles)]
        picks = [(lane % HEAD) == i * copies + lane // HEAD for i in range(tiles)]
        removed = dot(
            jnp.concatenate([(b * wide_direction).astype(BF16) for b in blocks], 0), ones
        )
        spread_values = dot(
            jnp.concatenate([jnp.where(p, wide_values, 0.0) for p in picks], 0).astype(BF16), ones
        )
        later = []
        for i in range(tiles):
            part = slice(i * heads, (i + 1) * heads)
            fresh = (
                blocks[i] * wide_decay
                - removed[part] * wide_learn
                + spread_values[part] * wide_keys
            )
            new_state[number, :, i * span : (i + 1) * span] = fresh
            later.append(fresh * wide_reader)
        read = split_sum(jnp.concatenate(later, 0), ones)
        gathered = jnp.where(picks[0], read[:heads], 0.0)
        for i in range(1, tiles):
            gathered = gathered + jnp.where(picks[i], read[i * heads : (i + 1) * heads], 0.0)
        readout = gathered[:, :HEAD]
        for i in range(1, copies):
            readout = readout + gathered[:, i * HEAD : (i + 1) * HEAD]
        centre = jnp.mean(readout, axis=-1, keepdims=True)
        spread = jnp.mean(jnp.square(readout - centre), axis=-1, keepdims=True)
        mixed[step * per_step + number] = (
            readout - centre
        ) * lax.rsqrt(spread + GROUP_EPS)

    @pl.when(step == steps - 1)
    def _():
        count = mixed.shape[0]
        channels = heads * HEAD
        flat = mixed[...].reshape(count * heads, HEAD)
        source = lax.broadcasted_iota(jnp.int32, (HEAD, channels), 0)
        target = lax.broadcasted_iota(jnp.int32, (HEAD, channels), 1)
        tiled = split_sum(flat, (target % HEAD == source).astype(F32).astype(BF16))
        head = lax.broadcasted_iota(jnp.int32, (count * heads, channels), 0) % heads
        channel = lax.broadcasted_iota(jnp.int32, (count * heads, channels), 1) // HEAD
        kept = (jnp.where(head == channel, tiled, 0.0) * head_gain[...]).astype(BF16)
        owner = lax.broadcasted_iota(jnp.int32, (count, count * heads), 1) // heads
        token = lax.broadcasted_iota(jnp.int32, (count, count * heads), 0)
        rows = dot((owner == token).astype(F32).astype(BF16), kept).astype(BF16)
        copy.wait()
        after = (tokens[...].astype(F32) + dot(rows, wbuf[...])).astype(BF16)
        residual[...] = after
        second[...] = rms_scale(after, second_gain[...]).astype(BF16)


def mixer(vectors, state, head_gain, tokens, w_output, second_gain):
    _, count, heads, _ = vectors.shape
    width = tokens.shape[1]
    entries = state.shape[2]
    per_step = 2 if count % 2 == 0 else 1
    steps = count // per_step
    whole = lambda array: pl.BlockSpec(array.shape, lambda i: (0,) * array.ndim)
    block = pl.BlockSpec((per_step, heads, entries), lambda i: (i, 0, 0))
    flat = pl.BlockSpec((count, width), lambda i: (0, 0))
    return pl.pallas_call(
        functools.partial(mixer_kernel, steps),
        grid=(steps,),
        out_shape=[
            jax.ShapeDtypeStruct(state.shape, F32),
            jax.ShapeDtypeStruct((count, width), BF16),
            jax.ShapeDtypeStruct((count, width), BF16),
        ],
        in_specs=[
            pl.BlockSpec((6, per_step, heads, HEAD), lambda i: (0, i, 0, 0)),
            block,
            whole(head_gain),
            flat,
            pl.BlockSpec(memory_space=pl.ANY),
            whole(second_gain),
        ],
        out_specs=[block, flat, flat],
        scratch_shapes=[
            pltpu.VMEM(w_output.shape, BF16),
            pltpu.VMEM((count, heads, HEAD), F32),
            pltpu.SemaphoreType.DMA,
        ],
        compiler_params=pltpu.CompilerParams(
            dimension_semantics=("arbitrary",), vmem_limit_bytes=VMEM_BYTES
        ),
        name="mixer",
    )(vectors, state, head_gain, tokens, w_output, second_gain)


def onehot(flags):
    return flags.astype(F32).astype(BF16)


def onehot_values(values):
    return values.astype(F32).astype(BF16)


def thirds(values):
    first = values.astype(BF16)
    rest = values - first.astype(F32)
    middle = rest.astype(BF16)
    return first, middle, (rest - middle.astype(F32)).astype(BF16)


def experts_kernel(
    devices,
    second,
    residual,
    routes,
    route_weights,
    shared_gate,
    shared_up,
    shared_down,
    expert_gate,
    expert_up,
    expert_down,
    out,
    sg,
    su,
    sd,
    eg,
    eu,
    ed,
    sbuf,
    rbuf,
    pbuf,
    abuf,
    xfull,
    local_sem,
    osend_sem,
    orecv_sem,
    bsend_sem,
    brecv_sem,
):
    count, width = second.shape
    part = width // PARTS
    block = PARTS * MOST
    total = devices * block
    tall = PARTS * count
    me = lax.axis_index("ep")
    barrier = pltpu.get_barrier_semaphore()

    def greet(offset, carry):
        pl.semaphore_signal(
            barrier, inc=1, device_id=((me + offset) % devices,), device_id_type=MESH
        )
        return carry

    lax.fori_loop(1, devices, greet, 0)
    loads = [
        pltpu.make_async_copy(source, target, local_sem.at[number])
        for number, (source, target) in enumerate(
            (
                (shared_gate, sg),
                (shared_up, su),
                (expert_gate.at[0], eg),
                (expert_up.at[0], eu),
                (shared_down, sd),
                (expert_down.at[0], ed),
            )
        )
    ]
    for load in loads:
        load.start()

    rows = second[...]
    lines = lax.broadcasted_iota(jnp.int32, (routes.shape[1], PARTS * count), 0)
    lanes = lax.broadcasted_iota(jnp.int32, (routes.shape[1], PARTS * count), 1)
    pick = onehot(lines == me * count + lanes % count)
    routes_wide = dot(onehot_values(routes[...]), pick)
    stacked = jnp.concatenate([rows[:, q * part : (q + 1) * part] for q in range(PARTS)], 0)
    line = lax.broadcasted_iota(jnp.int32, (total, tall), 0)
    lane = lax.broadcasted_iota(jnp.int32, (total, tall), 1)
    named = line < 0
    for j in range(TOPK):
        named = named | (routes_wide[j : j + 1, :] == (line // block).astype(F32))
    up_row = lax.broadcasted_iota(jnp.int32, (tall, tall), 0)
    up_col = lax.broadcasted_iota(jnp.int32, (tall, tall), 1)
    same = up_row // count == up_col // count
    before = dot(onehot(named), onehot(same & (up_row < up_col)))
    fits = (before == (line % MOST).astype(F32)) & (lane // count == (line % block) // MOST)
    outgoing = dot(onehot(named & fits), stacked).astype(BF16)
    sbuf[...] = outgoing.reshape(devices, block, part)
    pl.semaphore_wait(barrier, devices - 1)

    def exchange(source_ref, target_ref, send, receive, offset, landing):
        peer = (me + offset) % devices
        return pltpu.make_async_remote_copy(
            src_ref=source_ref.at[peer],
            dst_ref=target_ref.at[landing],
            send_sem=send.at[offset],
            recv_sem=receive.at[offset],
            device_id=(peer,),
            device_id_type=MESH,
        )

    def start_all(source_ref, target_ref, send, receive):
        def one(turn, carry):
            offset = devices // 2 + (1 - 2 * (turn % 2)) * ((turn + 1) // 2)
            exchange(source_ref, target_ref, send, receive, offset, me).start()
            return carry

        lax.fori_loop(0, devices - 1, one, 0)

    def receive_all(source_ref, target_ref, send, receive):
        def one(offset, carry):
            origin = (me + devices - offset) % devices
            exchange(source_ref, target_ref, send, receive, offset, origin).wait_recv()
            return carry

        lax.fori_loop(1, devices, one, 0)

    def sent_all(source_ref, target_ref, send, receive):
        def one(offset, carry):
            exchange(source_ref, target_ref, send, receive, offset, me).wait_send()
            return carry

        lax.fori_loop(1, devices, one, 0)

    there = (sbuf, rbuf, osend_sem, orecv_sem)
    back = (pbuf, abuf, bsend_sem, brecv_sem)
    start_all(*there)
    rbuf[me] = sbuf[me]

    def gated(inputs, gate_ref, up_ref):
        gate_part = dot(inputs, gate_ref[...])
        up_part = dot(inputs, up_ref[...])
        return (jax.nn.silu(gate_part) * up_part).astype(BF16)

    loads[0].wait()
    loads[1].wait()
    shared_hidden = gated(rows, sg, su)
    loads[4].wait()
    shared = dot(shared_hidden, sd[...])

    across = lax.broadcasted_iota(jnp.int32, (tall, total), 1)
    down = lax.broadcasted_iota(jnp.int32, (tall, total), 0)
    named_t = across < 0
    turned = (((1,), (1,)), ((), ()))
    lines_t = lax.broadcasted_iota(jnp.int32, (tall, routes.shape[1]), 1)
    lanes_t = lax.broadcasted_iota(jnp.int32, (tall, routes.shape[1]), 0)
    pick_t = onehot(lines_t == me * count + lanes_t % count)

    def picked(values):
        return lax.dot_general(pick_t, values, turned, preferred_element_type=F32)

    routes_tall = picked(onehot_values(routes[...]))
    weights_tall = sum(picked(piece) for piece in thirds(route_weights[...]))
    weight_t = jnp.zeros((tall, total), F32)
    for j in range(TOPK):
        hit = routes_tall[:, j : j + 1] == (across // block).astype(F32)
        named_t = named_t | hit
        weight_t = weight_t + jnp.where(hit, weights_tall[:, j : j + 1], 0.0)
    before_t = dot(onehot(same & (up_col < up_row)), onehot(named_t))
    fits_t = (before_t == (across % MOST).astype(F32)) & (
        down // count == (across % block) // MOST
    )
    weight_t = jnp.where(fits_t, weight_t, 0.0)
    first, middle, last = thirds(weight_t)

    slots = devices * MOST
    narrow = lax.broadcasted_iota(jnp.int32, (slots, total), 0)
    broad = lax.broadcasted_iota(jnp.int32, (slots, total), 1)
    tall_row = lax.broadcasted_iota(jnp.int32, (total, slots), 0)
    tall_col = lax.broadcasted_iota(jnp.int32, (total, slots), 1)
    takes = []
    gives = []
    for q in range(PARTS):
        takes.append(onehot(broad == narrow // MOST * block + q * MOST + narrow % MOST))
        gives.append(onehot(tall_row == tall_col // MOST * block + q * MOST + tall_col % MOST))

    receive_all(*there)
    received = rbuf[...].reshape(total, part)
    for q in range(PARTS):
        xfull[:, q * part : (q + 1) * part] = dot(takes[q], received).astype(BF16)
    loads[2].wait()
    loads[3].wait()
    hidden = gated(xfull[...], eg, eu)
    loads[5].wait()
    produced = jnp.zeros((total, part), F32)
    for q in range(PARTS):
        result = dot(hidden, ed[:, q * part : (q + 1) * part]).astype(BF16)
        produced = produced + dot(gives[q], result)
    pbuf[...] = produced.astype(BF16).reshape(devices, block, part)
    start_all(*back)
    abuf[me] = pbuf[me]
    receive_all(*back)
    answers = abuf[...].reshape(total, part)
    routed = dot(first, answers) + dot(middle, answers) + dot(last, answers)
    kept = residual[...].astype(F32) + shared
    for q in range(PARTS):
        cut = slice(q * part, (q + 1) * part)
        out[:, cut] = (kept[:, cut] + routed[q * count : (q + 1) * count]).astype(BF16)
    sent_all(*there)
    sent_all(*back)


def experts(devices, second, residual, routes, weights, *matrices):
    count, width = second.shape
    vmem = pl.BlockSpec(memory_space=pltpu.VMEM)
    hbm = pl.BlockSpec(memory_space=pl.ANY)
    dma = pltpu.SemaphoreType.DMA
    exchange = pltpu.VMEM((devices, PARTS * MOST, width // PARTS), BF16)
    return pl.pallas_call(
        functools.partial(experts_kernel, devices),
        out_shape=jax.ShapeDtypeStruct((count, width), BF16),
        in_specs=[vmem] * 4 + [hbm] * 6,
        out_specs=vmem,
        scratch_shapes=[pltpu.VMEM(m.shape[-2:], BF16) for m in matrices]
        + [exchange] * 4
        + [
            pltpu.VMEM((devices * MOST, width), BF16),
            dma((6,)),
            dma((devices,)),
            dma((devices,)),
            dma((devices,)),
            dma((devices,)),
        ],
        compiler_params=pltpu.CompilerParams(
            collective_id=1, has_side_effects=True, vmem_limit_bytes=VMEM_BYTES
        ),
        name="experts",
    )(second, residual, routes, weights, *matrices)


def per_device(
    tokens,
    recurrent_state,
    first_gain,
    w_receptance,
    w_key,
    w_value,
    decay_down,
    decay_up,
    decay_base,
    rate_down,
    rate_up,
    rate_base,
    key_scale,
    head_gain,
    w_output,
    second_gain,
    shared_gate,
    shared_up,
    shared_down,
    expert_gate,
    expert_up,
    expert_down,
    routes,
    route_weights,
):
    devices = lax.axis_size("ep")
    vectors = project(
        devices,
        tokens,
        first_gain[None, :],
        w_receptance,
        w_key,
        w_value,
        decay_down.T,
        decay_up,
        decay_base[None, :],
        rate_down.T,
        rate_up,
        rate_base[None, :],
        key_scale[None, :],
    )
    new_state, residual, second = mixer(
        vectors,
        recurrent_state,
        head_gain[None, :],
        tokens,
        w_output,
        second_gain[None, :],
    )
    new_tokens = experts(
        devices,
        second,
        residual,
        routes.T,
        route_weights.T,
        shared_gate,
        shared_up,
        shared_down,
        expert_gate,
        expert_up,
        expert_down,
    )
    return (new_tokens, new_state)


def solution(mesh):
    in_specs = (
        P("ep", None),
        P("ep", None, None),
        P(),
        P("ep", None),
        P("ep", None),
        P("ep", None),
        P(),
        P(),
        P(),
        P(),
        P(),
        P(),
        P(),
        P(),
        P(),
        P(),
        P(),
        P(),
        P(),
        P("ep", None, None),
        P("ep", None, None),
        P("ep", None, None),
        P(),
        P(),
    )
    out_specs = (P("ep", None), P("ep", None, None))
    return jax.shard_map(
        per_device, mesh=mesh, in_specs=in_specs, out_specs=out_specs, check_vma=False
    )
```

profile of v0, /device:TPU:1, one launch (start us, length us, event | category | flops | bytes accessed | tf_op | source)
XLA Modules:
  0.0 149.8 jit_solution(9288857390080107995)
XLA Ops:
  0.6 40.8 %project.1.vectors = f32[6,16,16,64]{3,2,1,0:T(8,128)} custom-call(bf16[16,2048]{1,0:T(8,128)(2,1)} %tokens.3, f32[1,2048]{1,0:T(1,128)} %bitcast.14, bf16[16,1024]{1,0:T(8,128)(2,1)} %w_r.1, bf16[16,1024]{1,0:T(8,128)(2,1)} %w_k.1, bf16[16,1024]{1,0:T(8,128)(2,1)} %w_v.1, bf16[64,2048]{1,0:T(8,128)(2,1)} %bitcast.10, bf16[64,1024]{1,0:T(8,128)(2,1)} %decay_up.1, ...), custom_call_target="tpu_custom_call" | custom-call | tf_op jit(solution)/shard_map/project/pallas_call | solution.py:257
  41.5 12.7 %mixer.1 = (f32[16,16,4096]{2,1,0:T(8,128)}, bf16[16,2048]{1,0:T(8,128)(2,1)}, bf16[16,2048]{1,0:T(8,128)(2,1)}) custom-call(f32[6,16,16,64]{3,2,1,0:T(8,128)} %project.1.vectors, f32[16,16,4096]{2,1,0:T(8,128)} %state.1, f32[1,1024]{1,0:T(1,128)} %bitcast.16, bf16[16,2048]{1,0:T(8,128)(2,1)} %tokens.3, bf16[1024,2048]{1,0:T(8,128)(2,1)} %w_output.1, ...), custom_call_target="tpu_custom_call" | custom-call | tf_op jit(solution)/shard_map/mixer/pallas_call | solution.py:394
  54.2 94.1 %experts.1 = bf16[16,2048]{1,0:T(8,128)(2,1)} custom-call(bf16[16,2048]{1,0:T(8,128)(2,1)} %get-tuple-element.5.second, bf16[16,2048]{1,0:T(8,128)(2,1)} %get-tuple-element.6.residual, s32[4,2048]{1,0:T(4,128)} %bitcast.12, f32[4,2048]{1,0:T(4,128)} %bitcast.13, bf16[2048,512]{1,0:T(8,128)(2,1)} %shared_gate.1, bf16[2048,512]{1,0:T(8,128)(2,1)} %shared_up.1, ...), custom_call_target="tpu_custom_call" | custom-call | tf_op jit(solution)/shard_map/experts/pallas_call | solution.py:637
  148.4 1.5 copy.27
where the time goes:
time: 150 us
  Pallas kernels  148 us (99%)
    pallas_call x1, Pallas kernels, experts(): pl.pallas_call(functools.partial(experts_kernel, devices), out_shape=jax....  94.1 us
    pallas_call x1, Pallas kernels, project(): pl.pallas_call(functools.partial(project_kernel, devices), out_shape=jax....  40.8 us
    pallas_call x1, Pallas kernels, mixer(): pl.pallas_call(functools.partial(mixer_kernel, steps), grid=(steps,), out...  12.7 us

commit v1 on v0

--- a/solution.py
+++ b/solution.py
@@ -11,7 +11,6 @@
 TOPK = 4
 MOST = 4
 GROUP = 8
-PARTS = 4
 NORM_EPS = 1e-06
 GROUP_EPS = 0.00064
 MESH = pl.DeviceIdType.MESH
@@ -428,15 +427,18 @@
     return values.astype(F32).astype(BF16)
 
 
-def thirds(values):
-    first = values.astype(BF16)
-    rest = values - first.astype(F32)
-    middle = rest.astype(BF16)
-    return first, middle, (rest - middle.astype(F32)).astype(BF16)
+RING = 4
+STRIDES = ((2, 8, 32), (8, 32, 2), (32, 2, 8))
+
+
+def part_widths(width):
+    tiles = width // 128
+    counts = [tiles // 3 + (1 if number < tiles % 3 else 0) for number in range(3)]
+    return [number * 128 for number in counts]
 
 
 def experts_kernel(
-    devices,
+    widths,
     second,
     residual,
     routes,
@@ -454,32 +456,39 @@
     eg,
     eu,
     ed,
-    sbuf,
-    rbuf,
-    pbuf,
-    abuf,
-    xfull,
-    local_sem,
-    osend_sem,
-    orecv_sem,
-    bsend_sem,
-    brecv_sem,
+    *rest,
 ):
-    count, width = second.shape
-    part = width // PARTS
-    block = PARTS * MOST
-    total = devices * block
-    tall = PARTS * count
+    near, chosen, inbox, answer, back, total, gather, line, final = [
+        rest[3 * i : 3 * i + 3] for i in range(9)
+    ]
+    local_sem = rest[27]
+    s1, r1, s2, r2, s3, r3, t3, u3, t2, u2, t1, u1 = rest[28:40]
+    count = second.shape[0]
+    tokens = routes.shape[1]
+    starts = [sum(widths[:p]) for p in range(3)]
+    cuts = [slice(starts[p], starts[p] + widths[p]) for p in range(3)]
+    blocks = RING * RING
+    plane = blocks * count
+    note = blocks * MOST
     me = lax.axis_index("ep")
+    core = me % 2
+    partner = me + 1 - 2 * core
+
+    def place(stride):
+        return (me // stride) % RING
+
+    def peer(stride, offset):
+        return me + ((place(stride) + offset) % RING - place(stride)) * stride
+
+    spots = [[place(stride) for stride in STRIDES[p]] for p in range(3)]
     barrier = pltpu.get_barrier_semaphore()
-
-    def greet(offset, carry):
-        pl.semaphore_signal(
-            barrier, inc=1, device_id=((me + offset) % devices,), device_id_type=MESH
-        )
-        return carry
-
-    lax.fori_loop(1, devices, greet, 0)
+    greet = [partner]
+    for stride in STRIDES[0]:
+        for offset in range(1, RING):
+            mate = peer(stride, offset)
+            greet = greet + [mate, mate + 1 - 2 * core]
+    for mate in greet:
+        pl.semaphore_signal(barrier, inc=1, device_id=(mate,), device_id_type=MESH)
     loads = [
         pltpu.make_async_copy(source, target, local_sem.at[number])
         for number, (source, target) in enumerate(
@@ -495,160 +504,338 @@
     ]
     for load in loads:
         load.start()
-
-    rows = second[...]
-    lines = lax.broadcasted_iota(jnp.int32, (routes.shape[1], PARTS * count), 0)
-    lanes = lax.broadcasted_iota(jnp.int32, (routes.shape[1], PARTS * count), 1)
-    pick = onehot(lines == me * count + lanes % count)
-    routes_wide = dot(onehot_values(routes[...]), pick)
-    stacked = jnp.concatenate([rows[:, q * part : (q + 1) * part] for q in range(PARTS)], 0)
-    line = lax.broadcasted_iota(jnp.int32, (total, tall), 0)
-    lane = lax.broadcasted_iota(jnp.int32, (total, tall), 1)
-    named = line < 0
-    for j in range(TOPK):
-        named = named | (routes_wide[j : j + 1, :] == (line // block).astype(F32))
-    up_row = lax.broadcasted_iota(jnp.int32, (tall, tall), 0)
-    up_col = lax.broadcasted_iota(jnp.int32, (tall, tall), 1)
-    same = up_row // count == up_col // count
-    before = dot(onehot(named), onehot(same & (up_row < up_col)))
-    fits = (before == (line % MOST).astype(F32)) & (lane // count == (line % block) // MOST)
-    outgoing = dot(onehot(named & fits), stacked).astype(BF16)
-    sbuf[...] = outgoing.reshape(devices, block, part)
-    pl.semaphore_wait(barrier, devices - 1)
-
-    def exchange(source_ref, target_ref, send, receive, offset, landing):
-        peer = (me + offset) % devices
+    pl.semaphore_wait(barrier, len(greet))
+
+    sends = []
+
+    def copy(source, target, send, receive, device):
         return pltpu.make_async_remote_copy(
-            src_ref=source_ref.at[peer],
-            dst_ref=target_ref.at[landing],
-            send_sem=send.at[offset],
-            recv_sem=receive.at[offset],
-            device_id=(peer,),
+            src_ref=source,
+            dst_ref=target,
+            send_sem=send,
+            recv_sem=receive,
+            device_id=(device,),
             device_id_type=MESH,
         )
 
-    def start_all(source_ref, target_ref, send, receive):
-        def one(turn, carry):
-            offset = devices // 2 + (1 - 2 * (turn % 2)) * ((turn + 1) // 2)
-            exchange(source_ref, target_ref, send, receive, offset, me).start()
-            return carry
-
-        lax.fori_loop(0, devices - 1, one, 0)
-
-    def receive_all(source_ref, target_ref, send, receive):
-        def one(offset, carry):
-            origin = (me + devices - offset) % devices
-            exchange(source_ref, target_ref, send, receive, offset, origin).wait_recv()
-            return carry
-
-        lax.fori_loop(1, devices, one, 0)
-
-    def sent_all(source_ref, target_ref, send, receive):
-        def one(offset, carry):
-            exchange(source_ref, target_ref, send, receive, offset, me).wait_send()
-            return carry
-
-        lax.fori_loop(1, devices, one, 0)
-
-    there = (sbuf, rbuf, osend_sem, orecv_sem)
-    back = (pbuf, abuf, bsend_sem, brecv_sem)
-    start_all(*there)
-    rbuf[me] = sbuf[me]
-
-    def gated(inputs, gate_ref, up_ref):
-        gate_part = dot(inputs, gate_ref[...])
-        up_part = dot(inputs, up_ref[...])
+    def launch(*args):
+        made = copy(*args)
+        made.start()
+        sends.append(made)
+
+    mine = [second.at[:, pl.ds(starts[p], widths[p])] for p in range(3)]
+
+    def onward(p, step, source):
+        a1, a2, _ = spots[p]
+        for offset in (1, 3, 2):
+            index = p * 16 + offset * 4 + step
+            launch(
+                source,
+                near[p].at[a2, (a1 + RING - step) % RING],
+                s2.at[index],
+                r2.at[index],
+                peer(STRIDES[p][1], offset),
+            )
+
+    for p in range(3):
+        a1, a2, _ = spots[p]
+        for offset in (1, 3, 2):
+            launch(
+                mine[p],
+                near[p].at[a2, a1],
+                s1.at[p * 4 + offset],
+                r1.at[p * 4 + offset],
+                peer(STRIDES[p][0], offset),
+            )
+    for p in range(3):
+        onward(p, 0, mine[p])
+    rows = second[...]
+    for p in range(3):
+        a1, a2, _ = spots[p]
+        near[p][a2, a1] = rows[:, cuts[p]]
+
+    def iota(shape, dim):
+        return lax.broadcasted_iota(jnp.int32, shape, dim)
+
+    def token_of(p, number):
+        first, second_stride, third = STRIDES[p]
+        device = (
+            spots[p][2] * third
+            + core
+            + number // (RING * count) * second_stride
+            + number // count % RING * first
+        )
+        return device * count + number % count
+
+    def expert_of(p, number):
+        third = STRIDES[p][2]
+        return me - spots[p][2] * third - core + number // 2 * third + number % 2
+
+    routes_low = onehot_values(routes[...])
+    weights_low = route_weights[...].astype(BF16)
+    up_row = iota((plane, plane), 0)
+    up_col = iota((plane, plane), 1)
+    same = up_row // count == up_col // count
+    upper = onehot(same & (up_row < up_col))
+    lower = onehot(same & (up_col < up_row))
+    slot_row = iota((note, plane), 0)
+    slot_col = iota((note, plane), 1)
+    wanted = jnp.where(slot_col // count == slot_row // MOST, slot_row % MOST, -2).astype(F32)
+    peers = 2 * RING
+
+    def selector(p):
+        pick = onehot(iota((tokens, plane), 0) == token_of(p, iota((tokens, plane), 1)))
+        here = dot(routes_low, pick)
+        names = expert_of(p, iota((peers, plane), 0)).astype(F32)
+        named = names < 0.0
+        for j in range(TOPK):
+            named = named | (here[j : j + 1, :] == names)
+        before = dot(onehot(named), upper)
+        rank = jnp.where(named, before, -1.0)
+        parts = [
+            onehot(jnp.broadcast_to(rank[i : i + 1, :], (note, plane)) == wanted)
+            for i in range(peers)
+        ]
+        return jnp.concatenate(parts, 0)
+
+    selectors = [selector(p) for p in range(3)]
+
+    for offset in (1, 3, 2):
+        for p in range(3):
+            a1, a2, _ = spots[p]
+            slot = near[p].at[a2, (a1 + RING - offset) % RING]
+            copy(mine[p], slot, s1.at[p * 4 + offset], r1.at[p * 4 + offset], partner).wait_recv()
+            onward(p, offset, slot)
+
+    for p in (1, 2, 0):
+        a1, a2, a3 = spots[p]
+        for offset in (1, 3, 2):
+            for step in (0, 1, 3, 2):
+                slot = near[p].at[(a2 + RING - offset) % RING, (a1 + RING - step) % RING]
+                index = p * 16 + offset * 4 + step
+                copy(mine[p], slot, s2.at[index], r2.at[index], partner).wait_recv()
+        held = near[p][...].reshape(plane, widths[p])
+        picked = dot(selectors[p], held).astype(BF16)
+        chosen[p][...] = picked.reshape(peers, note, widths[p])
+        for offset in (1, 3, 2):
+            chip = peer(STRIDES[p][2], offset) - core
+            for side in range(2):
+                launch(
+                    chosen[p].at[(a3 + offset) % RING * 2 + side],
+                    inbox[p].at[core, a3],
+                    s3.at[p * 8 + offset * 2 + side],
+                    r3.at[p * 8 + offset * 2 + core],
+                    chip + side,
+                )
+        launch(
+            chosen[p].at[a3 * 2 + 1 - core],
+            inbox[p].at[core, a3],
+            s3.at[p * 8],
+            r3.at[p * 8 + core],
+            partner,
+        )
+        inbox[p][core, a3] = chosen[p][a3 * 2 + core]
+
+    def gated(gate_part, up_part):
         return (jax.nn.silu(gate_part) * up_part).astype(BF16)
 
     loads[0].wait()
     loads[1].wait()
-    shared_hidden = gated(rows, sg, su)
+    shared_hidden = gated(dot(rows, sg[...]), dot(rows, su[...]))
     loads[4].wait()
-    shared = dot(shared_hidden, sd[...])
-
-    across = lax.broadcasted_iota(jnp.int32, (tall, total), 1)
-    down = lax.broadcasted_iota(jnp.int32, (tall, total), 0)
-    named_t = across < 0
+    kept = residual[...].astype(F32) + dot(shared_hidden, sd[...])
+
     turned = (((1,), (1,)), ((), ()))
-    lines_t = lax.broadcasted_iota(jnp.int32, (tall, routes.shape[1]), 1)
-    lanes_t = lax.broadcasted_iota(jnp.int32, (tall, routes.shape[1]), 0)
-    pick_t = onehot(lines_t == me * count + lanes_t % count)
-
-    def picked(values):
-        return lax.dot_general(pick_t, values, turned, preferred_element_type=F32)
-
-    routes_tall = picked(onehot_values(routes[...]))
-    weights_tall = sum(picked(piece) for piece in thirds(route_weights[...]))
-    weight_t = jnp.zeros((tall, total), F32)
-    for j in range(TOPK):
-        hit = routes_tall[:, j : j + 1] == (across // block).astype(F32)
-        named_t = named_t | hit
-        weight_t = weight_t + jnp.where(hit, weights_tall[:, j : j + 1], 0.0)
-    before_t = dot(onehot(same & (up_col < up_row)), onehot(named_t))
-    fits_t = (before_t == (across % MOST).astype(F32)) & (
-        down // count == (across % block) // MOST
-    )
-    weight_t = jnp.where(fits_t, weight_t, 0.0)
-    first, middle, last = thirds(weight_t)
-
-    slots = devices * MOST
-    narrow = lax.broadcasted_iota(jnp.int32, (slots, total), 0)
-    broad = lax.broadcasted_iota(jnp.int32, (slots, total), 1)
-    tall_row = lax.broadcasted_iota(jnp.int32, (total, slots), 0)
-    tall_col = lax.broadcasted_iota(jnp.int32, (total, slots), 1)
-    takes = []
-    gives = []
-    for q in range(PARTS):
-        takes.append(onehot(broad == narrow // MOST * block + q * MOST + narrow % MOST))
-        gives.append(onehot(tall_row == tall_col // MOST * block + q * MOST + tall_col % MOST))
-
-    receive_all(*there)
-    received = rbuf[...].reshape(total, part)
-    for q in range(PARTS):
-        xfull[:, q * part : (q + 1) * part] = dot(takes[q], received).astype(BF16)
+    tall_row = iota((plane, peers * note), 0)
+    tall_col = iota((plane, peers * note), 1)
+    expand = onehot(iota((128, peers * note), 0) == iota((128, peers * note), 1) // note)
+    wanted_t = jnp.where(
+        tall_row // count == tall_col % note // MOST, tall_col % MOST, -2
+    ).astype(F32)
+
+    def mixing(p):
+        pick = onehot(iota((plane, tokens), 1) == token_of(p, iota((plane, tokens), 0)))
+        here = lax.dot_general(pick, routes_low, turned, preferred_element_type=F32)
+        weigh = lax.dot_general(pick, weights_low, turned, preferred_element_type=F32)
+        number = iota((plane, 128), 1)
+        names = jnp.where(number < peers, expert_of(p, number), -1).astype(F32)
+        named = names < -2.0
+        weight = jnp.zeros((plane, 128), F32)
+        for j in range(TOPK):
+            hit = here[:, j : j + 1] == names
+            named = named | hit
+            weight = weight + jnp.where(hit, weigh[:, j : j + 1], 0.0)
+        before = dot(lower, onehot(named))
+        rank = dot(jnp.where(named, before, -1.0).astype(BF16), expand)
+        spread = dot(weight.astype(BF16), expand)
+        return jnp.where(rank == wanted_t, spread, 0.0).astype(BF16)
+
+    mixers = [mixing(p) for p in range(3)]
+
+    each = RING * note
+    turn_row = iota((each, each), 0)
+    turn_col = iota((each, each), 1)
+
+    def digits(number):
+        return number // 64, number // 16 % 4, number // 4 % 4, number % 4
+
+    def joined(a, b, c, d):
+        return ((a * RING + b) * RING + c) * MOST + d
+
+    def orders(number):
+        z, y, x, s = digits(number)
+        return [None, joined(x, z, y, s), joined(y, x, z, s)]
+
+    def restored(number):
+        first, middle, last, s = digits(number)
+        return [None, joined(middle, last, first, s), joined(last, first, middle, s)]
+
+    turns = [None] + [onehot(turn_col == orders(turn_row)[p]) for p in (1, 2)]
+    returns = [None] + [onehot(turn_col == restored(turn_row)[p]) for p in (1, 2)]
+
+    gate_part = None
+    up_part = None
     loads[2].wait()
     loads[3].wait()
-    hidden = gated(xfull[...], eg, eu)
+    for p in (1, 2, 0):
+        a3 = spots[p][2]
+        for offset in (0, 1, 3, 2):
+            for side in range(2):
+                if offset == 0 and side == 1:
+                    continue
+                which = side if offset else 1 - core
+                slot = inbox[p].at[which, (a3 + RING - offset) % RING]
+                index = p * 8 + offset * 2 + which
+                copy(chosen[p].at[0], slot, s3.at[index], r3.at[index], partner).wait_recv()
+        if p == 0:
+            inputs = inbox[p][...].reshape(2 * each, widths[p])
+        else:
+            inputs = jnp.concatenate(
+                [
+                    dot(turns[p], inbox[p][side].reshape(each, widths[p])).astype(BF16)
+                    for side in range(2)
+                ],
+                0,
+            )
+        gate_more = dot(inputs, eg[cuts[p], :])
+        up_more = dot(inputs, eu[cuts[p], :])
+        gate_part = gate_more if gate_part is None else gate_part + gate_more
+        up_part = up_more if up_part is None else up_part + up_more
+    hidden = gated(gate_part, up_part)
     loads[5].wait()
-    produced = jnp.zeros((total, part), F32)
-    for q in range(PARTS):
-        result = dot(hidden, ed[:, q * part : (q + 1) * part]).astype(BF16)
-        produced = produced + dot(gives[q], result)
-    pbuf[...] = produced.astype(BF16).reshape(devices, block, part)
-    start_all(*back)
-    abuf[me] = pbuf[me]
-    receive_all(*back)
-    answers = abuf[...].reshape(total, part)
-    routed = dot(first, answers) + dot(middle, answers) + dot(last, answers)
-    kept = residual[...].astype(F32) + shared
-    for q in range(PARTS):
-        cut = slice(q * part, (q + 1) * part)
-        out[:, cut] = (kept[:, cut] + routed[q * count : (q + 1) * count]).astype(BF16)
-    sent_all(*there)
-    sent_all(*back)
-
-
-def experts(devices, second, residual, routes, weights, *matrices):
+
+    for p in range(3):
+        a3 = spots[p][2]
+        if p == 0:
+            inputs = hidden
+        else:
+            inputs = jnp.concatenate(
+                [
+                    dot(returns[p], hidden[side * each : (side + 1) * each]).astype(BF16)
+                    for side in range(2)
+                ],
+                0,
+            )
+        result = dot(inputs, ed[:, cuts[p]]).astype(BF16)
+        answer[p][...] = result.reshape(2, RING, note, widths[p])
+        for offset in (1, 3, 2):
+            chip = peer(STRIDES[p][2], offset) - core
+            for side in range(2):
+                launch(
+                    answer[p].at[side, (a3 + offset) % RING],
+                    back[p].at[a3, core],
+                    t3.at[p * 8 + offset * 2 + side],
+                    u3.at[p * 8 + offset * 2 + core],
+                    chip + side,
+                )
+        launch(
+            answer[p].at[1 - core, a3],
+            back[p].at[a3, core],
+            t3.at[p * 8],
+            u3.at[p * 8 + core],
+            partner,
+        )
+        back[p][a3, core] = answer[p][core, a3]
+
+    for p in (1, 2, 0):
+        a1, a2, a3 = spots[p]
+        for offset in (0, 1, 3, 2):
+            for side in range(2):
+                if offset == 0 and side == 1:
+                    continue
+                which = side if offset else 1 - core
+                slot = back[p].at[(a3 + RING - offset) % RING, which]
+                index = p * 8 + offset * 2 + which
+                copy(chosen[p].at[0], slot, t3.at[index], u3.at[index], partner).wait_recv()
+        summed = dot(mixers[p], back[p][...].reshape(peers * note, widths[p])).astype(BF16)
+        total[p][...] = summed.reshape(RING, RING, count, widths[p])
+        for offset in (1, 3, 2):
+            launch(
+                total[p].at[(a2 + offset) % RING],
+                gather[p].at[offset],
+                t2.at[p * 4 + offset],
+                u2.at[p * 4 + offset],
+                peer(STRIDES[p][1], offset),
+            )
+    for p in (1, 2, 0):
+        a1, a2, a3 = spots[p]
+        summed = total[p][a2].astype(F32)
+        for offset in (1, 3, 2):
+            index = p * 4 + offset
+            slot = gather[p].at[offset]
+            copy(total[p].at[0], slot, t2.at[index], u2.at[index], partner).wait_recv()
+            summed = summed + gather[p][offset].astype(F32)
+        line[p][...] = summed.astype(BF16)
+        for offset in (1, 3, 2):
+            launch(
+                line[p].at[(a1 + offset) % RING],
+                final[p].at[offset],
+                t1.at[p * 4 + offset],
+                u1.at[p * 4 + offset],
+                peer(STRIDES[p][0], offset),
+            )
+    for p in (1, 2, 0):
+        a1 = spots[p][0]
+        summed = line[p][a1].astype(F32)
+        for offset in (1, 3, 2):
+            index = p * 4 + offset
+            slot = final[p].at[offset]
+            copy(line[p].at[0], slot, t1.at[index], u1.at[index], partner).wait_recv()
+            summed = summed + final[p][offset].astype(F32)
+        out[:, cuts[p]] = (kept[:, cuts[p]] + summed).astype(BF16)
+    for made in sends:
+        made.wait_send()
+
+
+def experts(second, residual, routes, weights, *matrices):
     count, width = second.shape
+    widths = part_widths(width)
     vmem = pl.BlockSpec(memory_space=pltpu.VMEM)
     hbm = pl.BlockSpec(memory_space=pl.ANY)
     dma = pltpu.SemaphoreType.DMA
-    exchange = pltpu.VMEM((devices, PARTS * MOST, width // PARTS), BF16)
+    blocks = RING * RING
+    note = blocks * MOST
+    shapes = (
+        (RING, RING, count),
+        (2 * RING, note),
+        (2, RING, note),
+        (2, RING, note),
+        (RING, 2, note),
+        (RING, RING, count),
+        (RING, RING, count),
+        (RING, count),
+        (RING, count),
+    )
+    shapes = [pltpu.VMEM(shape + (w,), BF16) for shape in shapes for w in widths]
+    sizes = (6, 12, 12, 48, 48, 24, 24, 24, 24, 12, 12, 12, 12)
     return pl.pallas_call(
-        functools.partial(experts_kernel, devices),
+        functools.partial(experts_kernel, widths),
         out_shape=jax.ShapeDtypeStruct((count, width), BF16),
         in_specs=[vmem] * 4 + [hbm] * 6,
         out_specs=vmem,
         scratch_shapes=[pltpu.VMEM(m.shape[-2:], BF16) for m in matrices]
-        + [exchange] * 4
-        + [
-            pltpu.VMEM((devices * MOST, width), BF16),
-            dma((6,)),
-            dma((devices,)),
-            dma((devices,)),
-            dma((devices,)),
-            dma((devices,)),
-        ],
+        + shapes
+        + [dma((size,)) for size in sizes],
         compiler_params=pltpu.CompilerParams(
             collective_id=1, has_side_effects=True, vmem_limit_bytes=VMEM_BYTES
         ),
@@ -707,7 +894,6 @@
         second_gain[None, :],
     )
     new_tokens = experts(
-        devices,
         second,
         residual,
         routes.T,

time: 150 us -> 108 us (0.72)
  Pallas kernels: 148 us -> 105 us
    pallas_call x1, Pallas kernels: 94.1 us -> 52 us  [experts(): pl.pallas_call(functools.partial(experts_kernel, widths), out_shape=jax.S...]
where the time goes in v1:
time: 108 us
  Pallas kernels  105 us (97%)
  local copies, waits for them, and re-layouts  1.47 us (1%)
    pallas_call x1, Pallas kernels, experts(): pl.pallas_call(functools.partial(experts_kernel, widths), out_shape=jax.S...  52 us
    pallas_call x1, Pallas kernels, project(): pl.pallas_call(functools.partial(project_kernel, devices), out_shape=jax....  40.8 us
    pallas_call x1, Pallas kernels, mixer(): pl.pallas_call(functools.partial(mixer_kernel, steps), grid=(steps,), out...  12.6 us

profile of v1, /device:TPU:1, one launch (start us, length us, event | category | flops | bytes accessed | tf_op | source)
XLA Modules:
  0.0 107.5 jit_solution(1755993016093975916)
XLA Ops:
  0.6 40.8 %project.1.vectors = f32[6,16,16,64]{3,2,1,0:T(8,128)} custom-call(bf16[16,2048]{1,0:T(8,128)(2,1)} %tokens.3, f32[1,2048]{1,0:T(1,128)} %bitcast.14, bf16[16,1024]{1,0:T(8,128)(2,1)} %w_r.1, bf16[16,1024]{1,0:T(8,128)(2,1)} %w_k.1, bf16[16,1024]{1,0:T(8,128)(2,1)} %w_v.1, bf16[64,2048]{1,0:T(8,128)(2,1)} %bitcast.10, bf16[64,1024]{1,0:T(8,128)(2,1)} %decay_up.1, ...), custom_call_target="tpu_custom_call" | custom-call | tf_op jit(solution)/shard_map/project/pallas_call | solution.py:256
  41.5 12.6 %mixer.1 = (f32[16,16,4096]{2,1,0:T(8,128)}, bf16[16,2048]{1,0:T(8,128)(2,1)}, bf16[16,2048]{1,0:T(8,128)(2,1)}) custom-call(f32[6,16,16,64]{3,2,1,0:T(8,128)} %project.1.vectors, f32[16,16,4096]{2,1,0:T(8,128)} %state.1, f32[1,1024]{1,0:T(1,128)} %bitcast.16, bf16[16,2048]{1,0:T(8,128)(2,1)} %tokens.3, bf16[1024,2048]{1,0:T(8,128)(2,1)} %w_output.1, ...), custom_call_target="tpu_custom_call" | custom-call | tf_op jit(solution)/shard_map/mixer/pallas_call | solution.py:393
  54.0 52.0 %experts.1 = bf16[16,2048]{1,0:T(8,128)(2,1)} custom-call(bf16[16,2048]{1,0:T(8,128)(2,1)} %get-tuple-element.5.second, bf16[16,2048]{1,0:T(8,128)(2,1)} %get-tuple-element.6.residual, s32[4,2048]{1,0:T(4,128)} %bitcast.12, f32[4,2048]{1,0:T(4,128)} %bitcast.13, bf16[2048,512]{1,0:T(8,128)(2,1)} %shared_gate.1, bf16[2048,512]{1,0:T(8,128)(2,1)} %shared_up.1, ...), custom_call_target="tpu_custom_call" | custom-call | tf_op jit(solution)/shard_map/experts/pallas_call | solution.py:831
  106.1 1.5 %copy.27 = bf16[16,2048]{1,0:T(8,128)(2,1)} copy(bf16[16,2048]{1,0:T(8,128)(2,1)} %experts.1) | data formatting | bytes 131072

commit v2 on v1

--- a/solution.py
+++ b/solution.py
@@ -10,7 +10,8 @@
 HEAD = 64
 TOPK = 4
 MOST = 4
-GROUP = 8
+RING = 4
+STRIDES = ((2, 8, 32), (8, 32, 2), (32, 2, 8))
 NORM_EPS = 1e-06
 GROUP_EPS = 0.00064
 MESH = pl.DeviceIdType.MESH
@@ -31,7 +32,6 @@
 
 
 def project_kernel(
-    devices,
     tokens,
     gain,
     w_r,
@@ -61,111 +61,154 @@
 ):
     rows, mix = w_r.shape
     half = mix // 2
-    count = tokens.shape[0]
-    groups = devices // GROUP
-    members = 2 * groups
-    depth = tokens.shape[1] // groups
+    count, width = tokens.shape
+    pair = 2 * rows
+    depth = width // RING
     me = lax.axis_index("ep")
-    base = (me // GROUP) * GROUP
-    place = me % GROUP
     core = me % 2
-    column = place // 2
-    member = (me // GROUP) * 2 + core
-    chip = me - core
-    x_bit = (place // 2) % 2
-    y_bit = place // 4
-    x_chip = chip + 2 - 4 * x_bit
-    y_chip = chip + 4 - 8 * y_bit
-    diag_chip = x_chip + 4 - 8 * y_bit
-    partner = chip + 1 - core
-
-    def peer_of(offset):
-        which = (member + offset) % members
-        return which, (which // 2) * GROUP + column * 2 + which % 2
-
+    partner = me + 1 - 2 * core
+
+    def place(stride):
+        return (me // stride) % RING
+
+    def peer(stride, offset):
+        return me + ((place(stride) + offset) % RING - place(stride)) * stride
+
+    spots = [[place(stride) for stride in STRIDES[p]] for p in range(3)]
     local = []
-    weights = (w_r, w_k, w_v)
-    for number, weight in enumerate(weights):
+    for p, weight in enumerate((w_r, w_k, w_v)):
         for side in range(2):
             local.append(
                 pltpu.make_async_copy(
                     weight.at[:, pl.ds(side * half, half)],
-                    stage.at[number, side],
-                    local_sem.at[number * 2 + side],
+                    stage.at[p, side],
+                    local_sem.at[p * 2 + side],
                 )
             )
     for copy in local:
         copy.start()
 
     barrier = pltpu.get_barrier_semaphore()
-    greet = [partner, x_chip, x_chip + 1, y_chip, y_chip + 1]
-    greet = greet + [peer_of(offset)[1] for offset in range(1, members)]
-    for peer in greet:
-        pl.semaphore_signal(barrier, inc=1, device_id=(peer,), device_id_type=MESH)
+    greet = [partner]
+    for stride in STRIDES[0]:
+        for offset in range(1, RING):
+            mate = peer(stride, offset)
+            greet = greet + [mate, mate + 1 - 2 * core]
+    for mate in greet:
+        pl.semaphore_signal(barrier, inc=1, device_id=(mate,), device_id_type=MESH)
 
     normed = rms_scale(tokens[...], gain[...]).astype(BF16)
-    for number in range(groups):
-        nsend[number] = normed[:, number * depth : (number + 1) * depth]
+    for q in range(RING):
+        nsend[0, q] = normed[:, q * depth : (q + 1) * depth]
+        chunks = [z * depth + y * RING * pair + q * pair for z in range(RING) for y in range(RING)]
+        nsend[1, q] = jnp.concatenate([normed[:, s : s + pair] for s in chunks], axis=1)
+        chunks = [z * depth + q * RING * pair for z in range(RING)]
+        nsend[2, q] = jnp.concatenate([normed[:, s : s + RING * pair] for s in chunks], axis=1)
     for copy in local:
         copy.wait()
     pl.semaphore_wait(barrier, len(greet))
 
-    def slot(number, device):
-        return wbuf.at[number, pl.ds(pl.multiple_of((device - base) * rows, rows), rows), :]
-
-    def weight_copy(number, source, landing, send, receive, target):
+    sends = []
+
+    def remote(source, target, send, receive, device):
         return pltpu.make_async_remote_copy(
             src_ref=source,
-            dst_ref=slot(number, landing),
-            send_sem=wsend_sem.at[number * 7 + send],
-            recv_sem=wrecv_sem.at[number * 7 + receive],
-            device_id=(target,),
+            dst_ref=target,
+            send_sem=send,
+            recv_sem=receive,
+            device_id=(device,),
             device_id_type=MESH,
         )
 
-    sends = []
-
-    def launch(copy):
-        copy.start()
-        sends.append(copy)
-
-    def direct(number):
-        for side in range(2):
-            source = stage.at[number, side]
-            launch(weight_copy(number, source, me, 1 + side, 1 + core, x_chip + side))
-            launch(weight_copy(number, source, me, 3 + side, 3 + core, y_chip + side))
-        launch(weight_copy(number, stage.at[number, 1 - core], me, 0, 0, partner))
-
-    def arrived(number, source, receive):
-        weight_copy(number, stage.at[0, 0], source, 0, receive, partner).wait_recv()
-
-    def relay(number):
-        arrived(number, y_chip, 3)
-        launch(weight_copy(number, slot(number, y_chip), y_chip, 5, 5, x_chip + core))
-        arrived(number, x_chip + 1, 2)
-        launch(weight_copy(number, slot(number, x_chip + 1), x_chip + 1, 6, 6, y_chip + core))
-
-    direct(0)
-    for offset in range(1, members):
-        which, device = peer_of(offset)
+    def launch(*args):
+        made = remote(*args)
+        made.start()
+        sends.append(made)
+
+    def chip_slot(p, first, second):
+        return wbuf.at[p, first, second] if p == 2 else wbuf.at[p, second, first]
+
+    def row_slot(p, first, second, which):
+        return chip_slot(p, first, second).at[which]
+
+    for p in range(3):
+        a1, a2, _ = spots[p]
+        for offset in (1, 3, 2):
+            chip = peer(STRIDES[p][0], offset) - core
+            for side in range(2):
+                launch(
+                    stage.at[p, side],
+                    row_slot(p, a1, a2, core),
+                    wsend_sem.at[p * 32 + offset * 2 + side],
+                    wrecv_sem.at[p * 32 + offset * 2 + core],
+                    chip + side,
+                )
         launch(
-            pltpu.make_async_remote_copy(
-                src_ref=nsend.at[which // 2],
-                dst_ref=xbuf.at[member],
-                send_sem=xsend_sem.at[offset],
-                recv_sem=xrecv_sem.at[offset],
-                device_id=(device,),
-                device_id_type=MESH,
-            )
-        )
-    direct(1)
-
-    for number in range(3):
-        own = stage[number, core]
-        wbuf[number, pl.ds(pl.multiple_of(place * rows, rows), rows), :] = own
-    xbuf[member] = nsend[me // GROUP]
-    relay(0)
-    direct(2)
+            stage.at[p, 1 - core],
+            row_slot(p, a1, a2, core),
+            wsend_sem.at[p * 32],
+            wrecv_sem.at[p * 32 + core],
+            partner,
+        )
+    for p in range(3):
+        a1, a2, _ = spots[p]
+        for offset in (1, 3, 2):
+            chip = peer(STRIDES[p][1], offset) - core
+            for side in range(2):
+                launch(
+                    stage.at[p, side],
+                    row_slot(p, a1, a2, core),
+                    wsend_sem.at[p * 32 + 8 + offset * 2 + side],
+                    wrecv_sem.at[p * 32 + 8 + offset * 2 + core],
+                    chip + side,
+                )
+    for p in range(3):
+        a3 = spots[p][2]
+        for offset in (1, 3, 2):
+            chip = peer(STRIDES[p][2], offset) - core
+            for side in range(2):
+                launch(
+                    nsend.at[p, (a3 + offset) % RING],
+                    xbuf.at[p, a3, core],
+                    xsend_sem.at[p * 8 + offset * 2 + side],
+                    xrecv_sem.at[p * 8 + offset * 2 + core],
+                    chip + side,
+                )
+        launch(
+            nsend.at[p, a3],
+            xbuf.at[p, a3, core],
+            xsend_sem.at[p * 8],
+            xrecv_sem.at[p * 8 + core],
+            partner,
+        )
+    for p in range(3):
+        a1, a2, a3 = spots[p]
+        own = stage[p, core]
+        if p == 2:
+            wbuf[p, a1, a2, core] = own
+        else:
+            wbuf[p, a2, a1, core] = own
+        xbuf[p, a3, core] = nsend[p, a3]
+
+    def arrived(p, slot, index):
+        remote(stage.at[p, 0], slot, wsend_sem.at[index], wrecv_sem.at[index], partner).wait_recv()
+
+    for step in (1, 3, 2):
+        for p in range(3):
+            a1, a2, _ = spots[p]
+            first = (a1 + RING - step) % RING
+            for which in range(2):
+                arrived(p, row_slot(p, first, a2, which), p * 32 + step * 2 + which)
+            block = chip_slot(p, first, a2)
+            for offset in (1, 3, 2):
+                index = p * 32 + 16 + offset * 4 + step
+                launch(
+                    block,
+                    block,
+                    wsend_sem.at[index],
+                    wrecv_sem.at[index],
+                    peer(STRIDES[p][1], offset),
+                )
 
     def put(number, values, first):
         for head in range(values.shape[1] // HEAD):
@@ -183,95 +226,109 @@
     rate_low = down(rate_down[...]).astype(BF16)
     put(4, jax.nn.sigmoid(rate_base[...] + dot(rate_low, rate_up[...])), 0)
 
-    for offset in range(1, members):
-        source = (member + members - offset) % members
-        pltpu.make_async_remote_copy(
-            src_ref=nsend.at[0],
-            dst_ref=xbuf.at[source],
-            send_sem=xsend_sem.at[offset],
-            recv_sem=xrecv_sem.at[offset],
-            device_id=(partner,),
-            device_id_type=MESH,
-        ).wait_recv()
-    stacked = xbuf[...].reshape(members * count, depth)
-
-    def part_copy(number, source, landing, offset, target):
-        return pltpu.make_async_remote_copy(
-            src_ref=psend.at[number, source],
-            dst_ref=precv.at[number, landing],
-            send_sem=psend_sem.at[number * members + offset],
-            recv_sem=precv_sem.at[number * members + offset],
-            device_id=(target,),
-            device_id_type=MESH,
-        )
-
-    def multiply(number):
-        arrived(number, partner, 0)
-        arrived(number, x_chip, 1)
-        arrived(number, y_chip + 1, 4)
-        arrived(number, diag_chip, 5)
-        arrived(number, diag_chip + 1, 6)
-        part = dot(stacked, wbuf[number]).astype(BF16)
-        psend[number] = part.reshape(members, count, half)
-        for offset in range(1, members):
-            which, device = peer_of(offset)
-            launch(part_copy(number, which, member, offset, device))
-        precv[number, member] = psend[number, member]
-
-    def finish(number):
-        for offset in range(1, members):
-            source = (member + members - offset) % members
-            part_copy(number, 0, source, offset, partner).wait_recv()
+    for p in range(3):
+        a1, a2, a3 = spots[p]
+        arrived(p, row_slot(p, a1, a2, 1 - core), p * 32 + 1 - core)
+        for offset in (0, 1, 3, 2):
+            for side in range(2):
+                if offset == 0 and side == 1:
+                    continue
+                which = side if offset else 1 - core
+                index = p * 8 + offset * 2 + which
+                remote(
+                    nsend.at[p, 0],
+                    xbuf.at[p, (a3 + RING - offset) % RING, which],
+                    xsend_sem.at[index],
+                    xrecv_sem.at[index],
+                    partner,
+                ).wait_recv()
+        for offset in (1, 3, 2):
+            second = (a2 + RING - offset) % RING
+            for which in range(2):
+                arrived(p, row_slot(p, a1, second, which), p * 32 + 8 + offset * 2 + which)
+            for step in (1, 3, 2):
+                block = chip_slot(p, (a1 + RING - step) % RING, second)
+                index = p * 32 + 16 + offset * 4 + step
+                remote(
+                    block, block, wsend_sem.at[index], wrecv_sem.at[index], partner
+                ).wait_recv()
+        stacked = xbuf[p].reshape(2 * RING * count, depth)
+        part = dot(stacked, wbuf[p].reshape(depth, half)).astype(BF16)
+        psend[p] = part.reshape(RING, 2, count, half)
+        for offset in (1, 3, 2):
+            chip = peer(STRIDES[p][2], offset) - core
+            for side in range(2):
+                launch(
+                    psend.at[p, (a3 + offset) % RING, side],
+                    precv.at[p, a3, core],
+                    psend_sem.at[p * 8 + offset * 2 + side],
+                    precv_sem.at[p * 8 + offset * 2 + core],
+                    chip + side,
+                )
+        launch(
+            psend.at[p, a3, 1 - core],
+            precv.at[p, a3, core],
+            psend_sem.at[p * 8],
+            precv_sem.at[p * 8 + core],
+            partner,
+        )
+        precv[p, a3, core] = psend[p, a3, core]
+
+    for p in range(3):
+        a3 = spots[p][2]
+        for offset in (0, 1, 3, 2):
+            for side in range(2):
+                if offset == 0 and side == 1:
+                    continue
+                which = side if offset else 1 - core
+                index = p * 8 + offset * 2 + which
+                remote(
+                    nsend.at[p, 0],
+                    precv.at[p, (a3 + RING - offset) % RING, which],
+                    psend_sem.at[index],
+                    precv_sem.at[index],
+                    partner,
+                ).wait_recv()
         for side in range(2):
-            total = precv[number, side].astype(F32)
-            for which in range(1, groups):
-                total = total + precv[number, which * 2 + side].astype(F32)
+            total = precv[p, 0, side].astype(F32)
+            for which in range(1, RING):
+                total = total + precv[p, which, side].astype(F32)
             total = total.astype(BF16).astype(F32)
-            put(number, total, side * (heads // 2))
-            if number == 1:
+            put(p, total, side * (heads // 2))
+            if p == 1:
                 scale = key_scale[:, side * half : (side + 1) * half]
                 put(5, total * scale, side * (heads // 2))
-
-    relay(1)
-    multiply(0)
-    relay(2)
-    multiply(1)
-    finish(0)
-    multiply(2)
-    finish(1)
-    finish(2)
-    for copy in sends:
-        copy.wait_send()
-
-
-def project(devices, tokens, gain, w_r, w_k, w_v, dd, du, db, rd, ru, rb, scale):
+    for made in sends:
+        made.wait_send()
+
+
+def project(tokens, gain, w_r, w_k, w_v, dd, du, db, rd, ru, rb, scale):
     count, width = tokens.shape
     rows, mix = w_r.shape
-    groups = devices // GROUP
-    members = 2 * groups
     half = mix // 2
+    depth = width // RING
     vmem = pl.BlockSpec(memory_space=pltpu.VMEM)
     hbm = pl.BlockSpec(memory_space=pl.ANY)
     dma = pltpu.SemaphoreType.DMA
     return pl.pallas_call(
-        functools.partial(project_kernel, devices),
+        project_kernel,
         out_shape=jax.ShapeDtypeStruct((6, count, mix // HEAD, HEAD), F32),
         in_specs=[vmem, vmem, hbm, hbm, hbm] + [vmem] * 7,
         out_specs=vmem,
         scratch_shapes=[
             pltpu.VMEM((3, 2, rows, half), BF16),
-            pltpu.VMEM((3, GROUP * rows, half), BF16),
-            pltpu.VMEM((groups, count, width // groups), BF16),
-            pltpu.VMEM((members, count, width // groups), BF16),
-            pltpu.VMEM((3, members, count, half), BF16),
-            pltpu.VMEM((3, members, count, half), BF16),
+            pltpu.VMEM((3, RING, RING, 2, rows, half), BF16),
+            pltpu.VMEM((3, RING, count, depth), BF16),
+            pltpu.VMEM((3, RING, 2, count, depth), BF16),
+            pltpu.VMEM((3, RING, 2, count, half), BF16),
+            pltpu.VMEM((3, RING, 2, count, half), BF16),
             dma((6,)),
-            dma((21,)),
-            dma((21,)),
-            dma((members,)),
-            dma((members,)),
-            dma((3 * members,)),
-            dma((3 * members,)),
+            dma((96,)),
+            dma((96,)),
+            dma((24,)),
+            dma((24,)),
+            dma((24,)),
+            dma((24,)),
         ],
         compiler_params=pltpu.CompilerParams(
             collective_id=0, has_side_effects=True, vmem_limit_bytes=VMEM_BYTES
@@ -427,10 +484,6 @@
     return values.astype(F32).astype(BF16)
 
 
-RING = 4
-STRIDES = ((2, 8, 32), (8, 32, 2), (32, 2, 8))
-
-
 def part_widths(width):
     tiles = width // 128
     counts = [tiles // 3 + (1 if number < tiles % 3 else 0) for number in range(3)]
@@ -869,9 +922,7 @@
     routes,
     route_weights,
 ):
-    devices = lax.axis_size("ep")
     vectors = project(
-        devices,
         tokens,
         first_gain[None, :],
         w_receptance,

time: 108 us -> 91.5 us (0.85)
  Pallas kernels: 105 us -> 88.9 us
    pallas_call x1, Pallas kernels: 40.8 us -> 29 us  [project(): pl.pallas_call(project_kernel, out_shape=jax.ShapeDtypeStruct((6, count,...]
    pallas_call x1, Pallas kernels: 52 us -> 47.3 us  [experts(): pl.pallas_call(functools.partial(experts_kernel, widths), out_shape=jax.S...]
where the time goes in v2:
time: 91.5 us; the launch traced here: 91 us
  Pallas kernels  88.9 us (97%)
  local copies, waits for them, and re-layouts  1.47 us (2%)
    pallas_call x1, Pallas kernels, experts(): pl.pallas_call(functools.partial(experts_kernel, widths), out_shape=jax.S...  47.3 us
    pallas_call x1, Pallas kernels, project(): pl.pallas_call(project_kernel, out_shape=jax.ShapeDtypeStruct((6, count,...  29 us
    pallas_call x1, Pallas kernels, mixer(): pl.pallas_call(functools.partial(mixer_kernel, steps), grid=(steps,), out...  12.6 us

profile of v2, /device:TPU:1, one launch (start us, length us, event | category | flops | bytes accessed | tf_op | source)
XLA Modules:
  0.0 91.0 jit_solution(17868990655951564021)
XLA Ops:
  0.6 29.0 %project.1.vectors = f32[6,16,16,64]{3,2,1,0:T(8,128)} custom-call(bf16[16,2048]{1,0:T(8,128)(2,1)} %tokens.3, f32[1,2048]{1,0:T(1,128)} %bitcast.14, bf16[16,1024]{1,0:T(8,128)(2,1)} %w_r.1, bf16[16,1024]{1,0:T(8,128)(2,1)} %w_k.1, bf16[16,1024]{1,0:T(8,128)(2,1)} %w_v.1, bf16[64,2048]{1,0:T(8,128)(2,1)} %bitcast.10, bf16[64,1024]{1,0:T(8,128)(2,1)} %decay_up.1, ...), custom_call_target="tpu_custom_call" | custom-call | tf_op jit(solution)/shard_map/project/pallas_call | solution.py:313
  29.7 12.6 %mixer.1 = (f32[16,16,4096]{2,1,0:T(8,128)}, bf16[16,2048]{1,0:T(8,128)(2,1)}, bf16[16,2048]{1,0:T(8,128)(2,1)}) custom-call(f32[6,16,16,64]{3,2,1,0:T(8,128)} %project.1.vectors, f32[16,16,4096]{2,1,0:T(8,128)} %state.1, f32[1,1024]{1,0:T(1,128)} %bitcast.16, bf16[16,2048]{1,0:T(8,128)(2,1)} %tokens.3, bf16[1024,2048]{1,0:T(8,128)(2,1)} %w_output.1, ...), custom_call_target="tpu_custom_call" | custom-call | tf_op jit(solution)/shard_map/mixer/pallas_call | solution.py:450
  42.3 47.3 %experts.1 = bf16[16,2048]{1,0:T(8,128)(2,1)} custom-call(bf16[16,2048]{1,0:T(8,128)(2,1)} %get-tuple-element.5.second, bf16[16,2048]{1,0:T(8,128)(2,1)} %get-tuple-element.6.residual, s32[4,2048]{1,0:T(4,128)} %bitcast.12, f32[4,2048]{1,0:T(4,128)} %bitcast.13, bf16[2048,512]{1,0:T(8,128)(2,1)} %shared_gate.1, bf16[2048,512]{1,0:T(8,128)(2,1)} %shared_up.1, ...), custom_call_target="tpu_custom_call" | custom-call | tf_op jit(solution)/shard_map/experts/pallas_call | solution.py:884
  89.6 1.5 %copy.27 = bf16[16,2048]{1,0:T(8,128)(2,1)} copy(bf16[16,2048]{1,0:T(8,128)(2,1)} %experts.1) | data formatting | bytes 131072

commit v3 on v2

--- a/solution.py
+++ b/solution.py
@@ -11,6 +11,7 @@
 TOPK = 4
 MOST = 4
 RING = 4
+SLICES = 6
 STRIDES = ((2, 8, 32), (8, 32, 2), (32, 2, 8))
 NORM_EPS = 1e-06
 GROUP_EPS = 0.00064
@@ -442,7 +443,7 @@
     _, count, heads, _ = vectors.shape
     width = tokens.shape[1]
     entries = state.shape[2]
-    per_step = 2 if count % 2 == 0 else 1
+    per_step = 8 if count % 8 == 0 else 1
     steps = count // per_step
     whole = lambda array: pl.BlockSpec(array.shape, lambda i: (0,) * array.ndim)
     block = pl.BlockSpec((per_step, heads, entries), lambda i: (i, 0, 0))
@@ -486,7 +487,7 @@
 
 def part_widths(width):
     tiles = width // 128
-    counts = [tiles // 3 + (1 if number < tiles % 3 else 0) for number in range(3)]
+    counts = [tiles // SLICES + (1 if number < tiles % SLICES else 0) for number in range(SLICES)]
     return [number * 128 for number in counts]
 
 
@@ -512,14 +513,14 @@
     *rest,
 ):
     near, chosen, inbox, answer, back, total, gather, line, final = [
-        rest[3 * i : 3 * i + 3] for i in range(9)
+        rest[SLICES * i : SLICES * (i + 1)] for i in range(9)
     ]
-    local_sem = rest[27]
-    s1, r1, s2, r2, s3, r3, t3, u3, t2, u2, t1, u1 = rest[28:40]
+    local_sem = rest[9 * SLICES]
+    s1, r1, s2, r2, s3, r3, t3, u3, t2, u2, t1, u1 = rest[9 * SLICES + 1 :]
     count = second.shape[0]
     tokens = routes.shape[1]
-    starts = [sum(widths[:p]) for p in range(3)]
-    cuts = [slice(starts[p], starts[p] + widths[p]) for p in range(3)]
+    starts = [sum(widths[:p]) for p in range(SLICES)]
+    cuts = [slice(starts[p], starts[p] + widths[p]) for p in range(SLICES)]
     blocks = RING * RING
     plane = blocks * count
     note = blocks * MOST
@@ -533,7 +534,8 @@
     def peer(stride, offset):
         return me + ((place(stride) + offset) % RING - place(stride)) * stride
 
-    spots = [[place(stride) for stride in STRIDES[p]] for p in range(3)]
+    strides = [STRIDES[p % 3] for p in range(SLICES)]
+    spots = [[place(stride) for stride in strides[p]] for p in range(SLICES)]
     barrier = pltpu.get_barrier_semaphore()
     greet = [partner]
     for stride in STRIDES[0]:
@@ -576,7 +578,7 @@
         made.start()
         sends.append(made)
 
-    mine = [second.at[:, pl.ds(starts[p], widths[p])] for p in range(3)]
+    mine = [second.at[:, pl.ds(starts[p], widths[p])] for p in range(SLICES)]
 
     def onward(p, step, source):
         a1, a2, _ = spots[p]
@@ -587,10 +589,10 @@
                 near[p].at[a2, (a1 + RING - step) % RING],
                 s2.at[index],
                 r2.at[index],
-                peer(STRIDES[p][1], offset),
+                peer(strides[p][1], offset),
             )
 
-    for p in range(3):
+    def enter(p):
         a1, a2, _ = spots[p]
         for offset in (1, 3, 2):
             launch(
@@ -598,12 +600,19 @@
                 near[p].at[a2, a1],
                 s1.at[p * 4 + offset],
                 r1.at[p * 4 + offset],
-                peer(STRIDES[p][0], offset),
+                peer(strides[p][0], offset),
             )
-    for p in range(3):
+
+    groups = [range(first, first + 3) for first in range(0, SLICES, 3)]
+    for p in groups[0]:
+        enter(p)
+    for p in groups[0]:
         onward(p, 0, mine[p])
+    for group in groups[1:]:
+        for p in group:
+            enter(p)
     rows = second[...]
-    for p in range(3):
+    for p in range(SLICES):
         a1, a2, _ = spots[p]
         near[p][a2, a1] = rows[:, cuts[p]]
 
@@ -611,7 +620,7 @@
         return lax.broadcasted_iota(jnp.int32, shape, dim)
 
     def token_of(p, number):
-        first, second_stride, third = STRIDES[p]
+        first, second_stride, third = strides[p]
         device = (
             spots[p][2] * third
             + core
@@ -621,7 +630,7 @@
         return device * count + number % count
 
     def expert_of(p, number):
-        third = STRIDES[p][2]
+        third = strides[p][2]
         return me - spots[p][2] * third - core + number // 2 * third + number % 2
 
     routes_low = onehot_values(routes[...])
@@ -653,14 +662,19 @@
 
     selectors = [selector(p) for p in range(3)]
 
-    for offset in (1, 3, 2):
-        for p in range(3):
-            a1, a2, _ = spots[p]
-            slot = near[p].at[a2, (a1 + RING - offset) % RING]
-            copy(mine[p], slot, s1.at[p * 4 + offset], r1.at[p * 4 + offset], partner).wait_recv()
-            onward(p, offset, slot)
-
-    for p in (1, 2, 0):
+    for group in groups:
+        if group != groups[0]:
+            for p in group:
+                onward(p, 0, mine[p])
+        for offset in (1, 3, 2):
+            for p in group:
+                a1, a2, _ = spots[p]
+                slot = near[p].at[a2, (a1 + RING - offset) % RING]
+                index = p * 4 + offset
+                copy(mine[p], slot, s1.at[index], r1.at[index], partner).wait_recv()
+                onward(p, offset, slot)
+
+    for p in range(SLICES):
         a1, a2, a3 = spots[p]
         for offset in (1, 3, 2):
             for step in (0, 1, 3, 2):
@@ -668,10 +682,10 @@
                 index = p * 16 + offset * 4 + step
                 copy(mine[p], slot, s2.at[index], r2.at[index], partner).wait_recv()
         held = near[p][...].reshape(plane, widths[p])
-        picked = dot(selectors[p], held).astype(BF16)
+        picked = dot(selectors[p % 3], held).astype(BF16)
         chosen[p][...] = picked.reshape(peers, note, widths[p])
         for offset in (1, 3, 2):
-            chip = peer(STRIDES[p][2], offset) - core
+            chip = peer(strides[p][2], offset) - core
             for side in range(2):
                 launch(
                     chosen[p].at[(a3 + offset) % RING * 2 + side],
@@ -692,6 +706,91 @@
     def gated(gate_part, up_part):
         return (jax.nn.silu(gate_part) * up_part).astype(BF16)
 
+    each = RING * note
+    turn_row = iota((each, each), 0)
+    turn_col = iota((each, each), 1)
+
+    def digits(number):
+        return number // 64, number // 16 % 4, number // 4 % 4, number % 4
+
+    def joined(a, b, c, d):
+        return ((a * RING + b) * RING + c) * MOST + d
+
+    def orders(number):
+        z, y, x, s = digits(number)
+        return [None, joined(x, z, y, s), joined(y, x, z, s)]
+
+    def restored(number):
+        first, middle, last, s = digits(number)
+        return [None, joined(middle, last, first, s), joined(last, first, middle, s)]
+
+    turns = [None] + [onehot(turn_col == orders(turn_row)[p]) for p in (1, 2)]
+    returns = [None] + [onehot(turn_col == restored(turn_row)[p]) for p in (1, 2)]
+
+    gate_part = None
+    up_part = None
+    loads[2].wait()
+    loads[3].wait()
+    for p in range(SLICES):
+        a3 = spots[p][2]
+        for offset in (0, 1, 3, 2):
+            for side in range(2):
+                if offset == 0 and side == 1:
+                    continue
+                which = side if offset else 1 - core
+                slot = inbox[p].at[which, (a3 + RING - offset) % RING]
+                index = p * 8 + offset * 2 + which
+                copy(chosen[p].at[0], slot, s3.at[index], r3.at[index], partner).wait_recv()
+        if p % 3 == 0:
+            inputs = inbox[p][...].reshape(2 * each, widths[p])
+        else:
+            inputs = jnp.concatenate(
+                [
+                    dot(turns[p % 3], inbox[p][side].reshape(each, widths[p])).astype(BF16)
+                    for side in range(2)
+                ],
+                0,
+            )
+        gate_more = dot(inputs, eg[cuts[p], :])
+        up_more = dot(inputs, eu[cuts[p], :])
+        gate_part = gate_more if gate_part is None else gate_part + gate_more
+        up_part = up_more if up_part is None else up_part + up_more
+    hidden = gated(gate_part, up_part)
+    loads[5].wait()
+
+    for p in range(SLICES):
+        a3 = spots[p][2]
+        if p % 3 == 0:
+            inputs = hidden
+        else:
+            inputs = jnp.concatenate(
+                [
+                    dot(returns[p % 3], hidden[side * each : (side + 1) * each]).astype(BF16)
+                    for side in range(2)
+                ],
+                0,
+            )
+        result = dot(inputs, ed[:, cuts[p]]).astype(BF16)
+        answer[p][...] = result.reshape(2, RING, note, widths[p])
+        for offset in (1, 3, 2):
+            chip = peer(strides[p][2], offset) - core
+            for side in range(2):
+                launch(
+                    answer[p].at[side, (a3 + offset) % RING],
+                    back[p].at[a3, core],
+                    t3.at[p * 8 + offset * 2 + side],
+                    u3.at[p * 8 + offset * 2 + core],
+                    chip + side,
+                )
+        launch(
+            answer[p].at[1 - core, a3],
+            back[p].at[a3, core],
+            t3.at[p * 8],
+            u3.at[p * 8 + core],
+            partner,
+        )
+        back[p][a3, core] = answer[p][core, a3]
+
     loads[0].wait()
     loads[1].wait()
     shared_hidden = gated(dot(rows, sg[...]), dot(rows, su[...]))
@@ -725,92 +824,7 @@
 
     mixers = [mixing(p) for p in range(3)]
 
-    each = RING * note
-    turn_row = iota((each, each), 0)
-    turn_col = iota((each, each), 1)
-
-    def digits(number):
-        return number // 64, number // 16 % 4, number // 4 % 4, number % 4
-
-    def joined(a, b, c, d):
-        return ((a * RING + b) * RING + c) * MOST + d
-
-    def orders(number):
-        z, y, x, s = digits(number)
-        return [None, joined(x, z, y, s), joined(y, x, z, s)]
-
-    def restored(number):
-        first, middle, last, s = digits(number)
-        return [None, joined(middle, last, first, s), joined(last, first, middle, s)]
-
-    turns = [None] + [onehot(turn_col == orders(turn_row)[p]) for p in (1, 2)]
-    returns = [None] + [onehot(turn_col == restored(turn_row)[p]) for p in (1, 2)]
-
-    gate_part = None
-    up_part = None
-    loads[2].wait()
-    loads[3].wait()
-    for p in (1, 2, 0):
-        a3 = spots[p][2]
-        for offset in (0, 1, 3, 2):
-            for side in range(2):
-                if offset == 0 and side == 1:
-                    continue
-                which = side if offset else 1 - core
-                slot = inbox[p].at[which, (a3 + RING - offset) % RING]
-                index = p * 8 + offset * 2 + which
-                copy(chosen[p].at[0], slot, s3.at[index], r3.at[index], partner).wait_recv()
-        if p == 0:
-            inputs = inbox[p][...].reshape(2 * each, widths[p])
-        else:
-            inputs = jnp.concatenate(
-                [
-                    dot(turns[p], inbox[p][side].reshape(each, widths[p])).astype(BF16)
-                    for side in range(2)
-                ],
-                0,
-            )
-        gate_more = dot(inputs, eg[cuts[p], :])
-        up_more = dot(inputs, eu[cuts[p], :])
-        gate_part = gate_more if gate_part is None else gate_part + gate_more
-        up_part = up_more if up_part is None else up_part + up_more
-    hidden = gated(gate_part, up_part)
-    loads[5].wait()
-
-    for p in range(3):
-        a3 = spots[p][2]
-        if p == 0:
-            inputs = hidden
-        else:
-            inputs = jnp.concatenate(
-                [
-                    dot(returns[p], hidden[side * each : (side + 1) * each]).astype(BF16)
-                    for side in range(2)
-                ],
-                0,
-            )
-        result = dot(inputs, ed[:, cuts[p]]).astype(BF16)
-        answer[p][...] = result.reshape(2, RING, note, widths[p])
-        for offset in (1, 3, 2):
-            chip = peer(STRIDES[p][2], offset) - core
-            for side in range(2):
-                launch(
-                    answer[p].at[side, (a3 + offset) % RING],
-                    back[p].at[a3, core],
-                    t3.at[p * 8 + offset * 2 + side],
-                    u3.at[p * 8 + offset * 2 + core],
-                    chip + side,
-                )
-        launch(
-            answer[p].at[1 - core, a3],
-            back[p].at[a3, core],
-            t3.at[p * 8],
-            u3.at[p * 8 + core],
-            partner,
-        )
-        back[p][a3, core] = answer[p][core, a3]
-
-    for p in (1, 2, 0):
+    for p in range(SLICES):
         a1, a2, a3 = spots[p]
         for offset in (0, 1, 3, 2):
             for side in range(2):
@@ -820,7 +834,7 @@
                 slot = back[p].at[(a3 + RING - offset) % RING, which]
                 index = p * 8 + offset * 2 + which
                 copy(chosen[p].at[0], slot, t3.at[index], u3.at[index], partner).wait_recv()
-        summed = dot(mixers[p], back[p][...].reshape(peers * note, widths[p])).astype(BF16)
+        summed = dot(mixers[p % 3], back[p][...].reshape(peers * note, widths[p])).astype(BF16)
         total[p][...] = summed.reshape(RING, RING, count, widths[p])
         for offset in (1, 3, 2):
             launch(
@@ -828,9 +842,9 @@
                 gather[p].at[offset],
                 t2.at[p * 4 + offset],
                 u2.at[p * 4 + offset],
-                peer(STRIDES[p][1], offset),
+                peer(strides[p][1], offset),
             )
-    for p in (1, 2, 0):
+    for p in range(SLICES):
         a1, a2, a3 = spots[p]
         summed = total[p][a2].astype(F32)
         for offset in (1, 3, 2):
@@ -845,9 +859,9 @@
                 final[p].at[offset],
                 t1.at[p * 4 + offset],
                 u1.at[p * 4 + offset],
-                peer(STRIDES[p][0], offset),
+                peer(strides[p][0], offset),
             )
-    for p in (1, 2, 0):
+    for p in range(SLICES):
         a1 = spots[p][0]
         summed = line[p][a1].astype(F32)
         for offset in (1, 3, 2):
@@ -880,7 +894,7 @@
         (RING, count),
     )
     shapes = [pltpu.VMEM(shape + (w,), BF16) for shape in shapes for w in widths]
-    sizes = (6, 12, 12, 48, 48, 24, 24, 24, 24, 12, 12, 12, 12)
+    sizes = [6] + [SLICES * size for size in (4, 4, 16, 16, 8, 8, 8, 8, 4, 4, 4, 4)]
     return pl.pallas_call(
         functools.partial(experts_kernel, widths),
         out_shape=jax.ShapeDtypeStruct((count, width), BF16),

time: 91.5 us -> 86.6 us (0.946)
  Pallas kernels: 88.9 us -> 84.2 us
    pallas_call x1, Pallas kernels: 12.6 us -> 8.29 us  [mixer(): pl.pallas_call(functools.partial(mixer_kernel, steps), grid=(steps,), out...]
where the time goes in v3:
time: 86.6 us; the launch traced here: 86.3 us
  Pallas kernels  84.2 us (97%)
  local copies, waits for them, and re-layouts  1.47 us (2%)
    pallas_call x1, Pallas kernels, experts(): pl.pallas_call(functools.partial(experts_kernel, widths), out_shape=jax.S...  46.9 us
    pallas_call x1, Pallas kernels, project(): pl.pallas_call(project_kernel, out_shape=jax.ShapeDtypeStruct((6, count,...  29 us
    pallas_call x1, Pallas kernels, mixer(): pl.pallas_call(functools.partial(mixer_kernel, steps), grid=(steps,), out...  8.29 us

profile of v3, /device:TPU:1, one launch (start us, length us, event | category | flops | bytes accessed | tf_op | source)
XLA Modules:
  0.0 86.3 jit_solution(9301137449021784056)
XLA Ops:
  0.6 29.0 %project.1.vectors = f32[6,16,16,64]{3,2,1,0:T(8,128)} custom-call(bf16[16,2048]{1,0:T(8,128)(2,1)} %tokens.3, f32[1,2048]{1,0:T(1,128)} %bitcast.14, bf16[16,1024]{1,0:T(8,128)(2,1)} %w_r.1, bf16[16,1024]{1,0:T(8,128)(2,1)} %w_k.1, bf16[16,1024]{1,0:T(8,128)(2,1)} %w_v.1, bf16[64,2048]{1,0:T(8,128)(2,1)} %bitcast.10, bf16[64,1024]{1,0:T(8,128)(2,1)} %decay_up.1, ...), custom_call_target="tpu_custom_call" | custom-call | tf_op jit(solution)/shard_map/project/pallas_call | solution.py:314
  29.7 8.3 %mixer.1 = (f32[16,16,4096]{2,1,0:T(8,128)}, bf16[16,2048]{1,0:T(8,128)(2,1)}, bf16[16,2048]{1,0:T(8,128)(2,1)}) custom-call(f32[6,16,16,64]{3,2,1,0:T(8,128)} %project.1.vectors, f32[16,16,4096]{2,1,0:T(8,128)} %state.1, f32[1,1024]{1,0:T(1,128)} %bitcast.16, bf16[16,2048]{1,0:T(8,128)(2,1)} %tokens.3, bf16[1024,2048]{1,0:T(8,128)(2,1)} %w_output.1, ...), custom_call_target="tpu_custom_call" | custom-call | tf_op jit(solution)/shard_map/mixer/pallas_call | solution.py:451
  38.0 46.9 %experts.1 = bf16[16,2048]{1,0:T(8,128)(2,1)} custom-call(bf16[16,2048]{1,0:T(8,128)(2,1)} %get-tuple-element.5.second, bf16[16,2048]{1,0:T(8,128)(2,1)} %get-tuple-element.6.residual, s32[4,2048]{1,0:T(4,128)} %bitcast.12, f32[4,2048]{1,0:T(4,128)} %bitcast.13, bf16[2048,512]{1,0:T(8,128)(2,1)} %shared_gate.1, bf16[2048,512]{1,0:T(8,128)(2,1)} %shared_up.1, ...), custom_call_target="tpu_custom_call" | custom-call | tf_op jit(solution)/shard_map/experts/pallas_call | solution.py:898
  84.9 1.5 %copy.27 = bf16[16,2048]{1,0:T(8,128)(2,1)} copy(bf16[16,2048]{1,0:T(8,128)(2,1)} %experts.1) | data formatting | bytes 131072

commit v4 on v3

v4 whole, which is shorter than its diff:
```python
import functools

import jax
import jax.numpy as jnp
from jax import lax
from jax.experimental import pallas as pl
from jax.experimental.pallas import tpu as pltpu
from jax.sharding import PartitionSpec as P

HEAD = 64
TOPK = 4
MOST = 4
RING = 4
SLICES = 6
STRIDES = ((2, 8, 32), (8, 32, 2), (32, 2, 8))
NORM_EPS = 1e-06
GROUP_EPS = 0.00064
MESH = pl.DeviceIdType.MESH
F32 = jnp.float32
BF16 = jnp.bfloat16
VMEM_BYTES = 60 * 1024 * 1024


def dot(a, b):
    return jnp.dot(a, b, preferred_element_type=F32)


def rms_scale(inputs, gain):
    widened = inputs.astype(F32)
    return (
        widened * lax.rsqrt(jnp.mean(widened * widened, axis=-1, keepdims=True) + NORM_EPS) * gain
    )


def onehot(flags):
    return flags.astype(F32).astype(BF16)


def onehot_values(values):
    return values.astype(F32).astype(BF16)


def part_widths(width):
    tiles = width // 128
    counts = [tiles // SLICES + (1 if number < tiles % SLICES else 0) for number in range(SLICES)]
    return [number * 128 for number in counts]


def layer_kernel(
    widths,
    tokens,
    gain,
    decay_down,
    decay_up,
    decay_base,
    rate_down,
    rate_up,
    rate_base,
    key_scale,
    head_gain,
    second_gain,
    routes,
    route_weights,
    w_r,
    w_k,
    w_v,
    state,
    w_output,
    shared_gate,
    shared_up,
    shared_down,
    expert_gate,
    expert_up,
    expert_down,
    out,
    wide_out,
    low_out,
    stage,
    wbuf,
    nsend,
    xbuf,
    psend,
    precv,
    vecs,
    old,
    wo,
    sg,
    su,
    sd,
    eg,
    eu,
    ed,
    fold,
    second,
    selectors,
    mixers,
    *rest,
):
    near, chosen, inbox, answer, back, total, gather, line, final = [
        rest[SLICES * i : SLICES * (i + 1)] for i in range(9)
    ]
    local_sem, load_sem = rest[9 * SLICES : 9 * SLICES + 2]
    wsend_sem, wrecv_sem, xsend_sem, xrecv_sem, psend_sem, precv_sem = rest[
        9 * SLICES + 2 : 9 * SLICES + 8
    ]
    s1, r1, r2, s3, r3, t3, u3, t2, u2, t1, u1 = rest[9 * SLICES + 8 :]
    rows, mix = w_r.shape
    half = mix // 2
    count, width = tokens.shape
    pair = 2 * rows
    depth = width // RING
    me = lax.axis_index("ep")
    core = me % 2
    partner = me + 1 - 2 * core

    def place(stride):
        return (me // stride) % RING

    def peer(stride, offset):
        return me + ((place(stride) + offset) % RING - place(stride)) * stride

    spots = [[place(stride) for stride in STRIDES[p % 3]] for p in range(SLICES)]
    local = []
    for p, weight in enumerate((w_r, w_k, w_v)):
        for side in range(2):
            local.append(
                pltpu.make_async_copy(
                    weight.at[:, pl.ds(side * half, half)],
                    stage.at[p, side],
                    local_sem,
                )
            )
    for copy in local:
        copy.start()

    barrier = pltpu.get_barrier_semaphore()
    greet = [partner]
    for stride in STRIDES[0]:
        for offset in range(1, RING):
            mate = peer(stride, offset)
            greet = greet + [mate, mate + 1 - 2 * core]
    for mate in greet:
        pl.semaphore_signal(barrier, inc=1, device_id=(mate,), device_id_type=MESH)

    loads = [
        pltpu.make_async_copy(source, target, load_sem.at[number])
        for number, (source, target) in enumerate(
            (
                (shared_gate, sg),
                (shared_up, su),
                (expert_gate.at[0], eg),
                (expert_up.at[0], eu),
                (shared_down, sd),
                (expert_down.at[0], ed),
                (state, old),
                (w_output, wo),
            )
        )
    ]
    for number in (6, 7, 2, 3, 5, 0, 1, 4):
        loads[number].start()

    normed = rms_scale(tokens[...], gain[...]).astype(BF16)
    for q in range(RING):
        nsend[0, q] = normed[:, q * depth : (q + 1) * depth]
        chunks = [z * depth + y * RING * pair + q * pair for z in range(RING) for y in range(RING)]
        nsend[1, q] = jnp.concatenate([normed[:, s : s + pair] for s in chunks], axis=1)
        chunks = [z * depth + q * RING * pair for z in range(RING)]
        nsend[2, q] = jnp.concatenate([normed[:, s : s + RING * pair] for s in chunks], axis=1)
    def remote(source, target, send, receive, device):
        return pltpu.make_async_remote_copy(
            src_ref=source,
            dst_ref=target,
            send_sem=send,
            recv_sem=receive,
            device_id=(device,),
            device_id_type=MESH,
        )

    def launch(*args):
        remote(*args).start()

    def settle(view, semaphore):
        remote(view, view, semaphore, semaphore, partner).wait_recv()

    def chip_index(p, first, second):
        return first * RING + second if p == 2 else second * RING + first

    def row_slot(p, first, second, which):
        return wbuf.at[p, chip_index(p, first, second) * 2 + which]

    settle(stage, local_sem)
    pl.semaphore_wait(barrier, len(greet))

    for p in range(3):
        a1, a2, _ = spots[p]
        for offset in (1, 3, 2):
            chip = peer(STRIDES[p][0], offset) - core
            for side in range(2):
                launch(
                    stage.at[p, side],
                    row_slot(p, a1, a2, core),
                    wsend_sem.at[p],
                    wrecv_sem.at[p * RING + offset],
                    chip + side,
                )
        launch(
            stage.at[p, 1 - core],
            row_slot(p, a1, a2, core),
            wsend_sem.at[p],
            wrecv_sem.at[p * RING],
            partner,
        )
    for p in range(3):
        a1, a2, _ = spots[p]
        for offset in (1, 3, 2):
            chip = peer(STRIDES[p][1], offset) - core
            for side in range(2):
                launch(
                    stage.at[p, side],
                    row_slot(p, a1, a2, core),
                    wsend_sem.at[p],
                    wrecv_sem.at[p * RING],
                    chip + side,
                )
    for p in range(3):
        a3 = spots[p][2]
        for offset in (1, 3, 2):
            chip = peer(STRIDES[p][2], offset) - core
            for side in range(2):
                launch(
                    nsend.at[p, (a3 + offset) % RING],
                    xbuf.at[p, a3 * 2 + core],
                    xsend_sem.at[p],
                    xrecv_sem.at[p],
                    chip + side,
                )
        launch(
            nsend.at[p, a3],
            xbuf.at[p, a3 * 2 + core],
            xsend_sem.at[p],
            xrecv_sem.at[p],
            partner,
        )
    for p in range(3):
        a1, a2, a3 = spots[p]
        own = stage[p, core]
        wbuf[p, chip_index(p, a1, a2) * 2 + core] = own
        xbuf[p, a3 * 2 + core] = nsend[p, a3]

    for step in (1, 3, 2):
        for p in range(3):
            a1, a2, _ = spots[p]
            first = (a1 + RING - step) % RING
            block = wbuf.at[p, pl.ds(chip_index(p, first, a2) * 2, 2)]
            settle(block, wrecv_sem.at[p * RING + step])
            for offset in (1, 3, 2):
                launch(
                    block,
                    block,
                    wsend_sem.at[p],
                    wrecv_sem.at[p * RING],
                    peer(STRIDES[p][1], offset),
                )

    def put(number, values, first):
        for head in range(values.shape[1] // HEAD):
            vecs[number, :, first + head, :] = values[:, head * HEAD : (head + 1) * HEAD]

    heads = mix // HEAD
    flip = (((1,), (1,)), ((), ()))

    def down(matrix):
        return lax.dot_general(normed, matrix, flip, preferred_element_type=F32)

    decay_low = jnp.tanh(down(decay_down[...])).astype(BF16)
    decay_pre = decay_base[...] + dot(decay_low, decay_up[...])
    put(3, jnp.exp(-jnp.exp(-jax.nn.softplus(-decay_pre) - 0.5)), 0)
    rate_low = down(rate_down[...]).astype(BF16)
    put(4, jax.nn.sigmoid(rate_base[...] + dot(rate_low, rate_up[...])), 0)

    strides = [STRIDES[p % 3] for p in range(SLICES)]
    note = RING * RING * MOST
    plane = RING * RING * count
    every = routes.shape[1]
    entries = old.shape[2]

    def iota(shape, dim):
        return lax.broadcasted_iota(jnp.int32, shape, dim)

    def token_of(p, number):
        first, second_stride, third = strides[p]
        device = (
            spots[p][2] * third
            + core
            + number // (RING * count) * second_stride
            + number // count % RING * first
        )
        return device * count + number % count

    def expert_of(p, number):
        third = strides[p][2]
        return me - spots[p][2] * third - core + number // 2 * third + number % 2

    routes_low = onehot_values(routes[...])
    weights_low = route_weights[...].astype(BF16)
    up_row = iota((plane, plane), 0)
    up_col = iota((plane, plane), 1)
    same = up_row // count == up_col // count
    upper = onehot(same & (up_row < up_col))
    lower = onehot(same & (up_col < up_row))
    slot_row = iota((note, plane), 0)
    slot_col = iota((note, plane), 1)
    wanted = jnp.where(slot_col // count == slot_row // MOST, slot_row % MOST, -2).astype(F32)
    peers = 2 * RING

    def selector(p):
        pick = onehot(iota((every, plane), 0) == token_of(p, iota((every, plane), 1)))
        here = dot(routes_low, pick)
        names = expert_of(p, iota((peers, plane), 0)).astype(F32)
        named = names < 0.0
        for j in range(TOPK):
            named = named | (here[j : j + 1, :] == names)
        before = dot(onehot(named), upper)
        rank = jnp.where(named, before, -1.0)
        parts = [
            onehot(jnp.broadcast_to(rank[i : i + 1, :], (note, plane)) == wanted)
            for i in range(peers)
        ]
        return jnp.concatenate(parts, 0)

    for p in range(3):
        selectors[p] = selector(p)

    fold[...] = onehot(iota((entries, HEAD), 0) // HEAD == iota((entries, HEAD), 1))
    each = RING * note
    turn_row = iota((each, each), 0)
    turn_col = iota((each, each), 1)

    def digits(number):
        return number // 64, number // 16 % 4, number // 4 % 4, number % 4

    def joined(a, b, c, d):
        return ((a * RING + b) * RING + c) * MOST + d

    def orders(number):
        z, y, x, s = digits(number)
        return [None, joined(x, z, y, s), joined(y, x, z, s)]

    def restored(number):
        first, middle, last, s = digits(number)
        return [None, joined(middle, last, first, s), joined(last, first, middle, s)]

    turns = [None] + [onehot(turn_col == orders(turn_row)[p]) for p in (1, 2)]
    returns = [None] + [onehot(turn_col == restored(turn_row)[p]) for p in (1, 2)]

    for p in range(3):
        a1, a2, a3 = spots[p]
        settle(xbuf.at[p, pl.ds(0, 7)], xrecv_sem.at[p])
        settle(wbuf.at[p, pl.ds(0, 25)], wrecv_sem.at[p * RING])
        stacked = xbuf[p].reshape(2 * RING * count, depth)
        part = dot(stacked, wbuf[p].reshape(depth, half)).astype(BF16)
        psend[p] = part.reshape(2 * RING, count, half)
        for offset in (1, 3, 2):
            chip = peer(STRIDES[p][2], offset) - core
            for side in range(2):
                launch(
                    psend.at[p, (a3 + offset) % RING * 2 + side],
                    precv.at[p, a3 * 2 + core],
                    psend_sem.at[p],
                    precv_sem.at[p],
                    chip + side,
                )
        launch(
            psend.at[p, a3 * 2 + 1 - core],
            precv.at[p, a3 * 2 + core],
            psend_sem.at[p],
            precv_sem.at[p],
            partner,
        )
        precv[p, a3 * 2 + core] = psend[p, a3 * 2 + core]

    for p in range(3):
        settle(precv.at[p, pl.ds(0, 7)], precv_sem.at[p])
        for side in range(2):
            added = precv[p, side].astype(F32)
            for which in range(1, RING):
                added = added + precv[p, which * 2 + side].astype(F32)
            added = added.astype(BF16).astype(F32)
            put(p, added, side * (heads // 2))
            if p == 1:
                scale = key_scale[:, side * half : (side + 1) * half]
                put(5, added * scale, side * (heads // 2))

    tall = count * heads
    reader, keys, values, decay, learn, scaled = [vecs[w].reshape(tall, HEAD) for w in range(6)]
    direction = scaled / jnp.sqrt(jnp.sum(scaled * scaled, axis=-1, keepdims=True) + 1.0)
    learned = direction * learn

    def twice(inputs):
        return jnp.concatenate([inputs, inputs], axis=1)

    along = twice(direction)
    reading = twice(decay * reader)
    loads[6].wait()
    cells = [
        old[:, :, lane : lane + 2 * HEAD].reshape(tall, 2 * HEAD)
        for lane in range(0, entries, 2 * HEAD)
    ]
    removed = dot(jnp.concatenate([(c * along).astype(BF16) for c in cells], 1), fold[...])
    readout = dot(jnp.concatenate([(c * reading).astype(BF16) for c in cells], 1), fold[...])
    readout = (
        readout
        - removed * jnp.sum(learned * reader, axis=-1, keepdims=True)
        + values * jnp.sum(keys * reader, axis=-1, keepdims=True)
    )
    centre = jnp.mean(readout, axis=-1, keepdims=True)
    spread = jnp.mean(jnp.square(readout - centre), axis=-1, keepdims=True)
    mixed = (readout - centre) * lax.rsqrt(spread + GROUP_EPS)
    vecs[5] = mixed.reshape(count, heads, HEAD)
    flat = jnp.concatenate([vecs[5, :, head, :] for head in range(heads)], axis=1)
    flat = (flat * head_gain[...]).astype(BF16)
    loads[7].wait()
    after = (tokens[...].astype(F32) + dot(flat, wo[...])).astype(BF16)
    second[...] = rms_scale(after, second_gain[...]).astype(BF16)

    starts = [sum(widths[:p]) for p in range(SLICES)]
    cuts = [slice(starts[p], starts[p] + widths[p]) for p in range(SLICES)]
    mine = [second.at[:, pl.ds(starts[p], widths[p])] for p in range(SLICES)]

    def onward(p, step, source):
        a1, a2, _ = spots[p]
        for offset in (1, 3, 2):
            launch(
                source,
                near[p].at[a2 * RING + (a1 + RING - step) % RING],
                s1.at[p],
                r2.at[p],
                peer(strides[p][1], offset),
            )

    def enter(p):
        a1, a2, _ = spots[p]
        for offset in (1, 3, 2):
            launch(
                mine[p],
                near[p].at[a2 * RING + a1],
                s1.at[p],
                r1.at[p * 3 + offset - 1],
                peer(strides[p][0], offset),
            )

    groups = [range(first, first + 3) for first in range(0, SLICES, 3)]
    for p in groups[0]:
        enter(p)
    for p in groups[0]:
        onward(p, 0, mine[p])
    for group in groups[1:]:
        for p in group:
            enter(p)
    sent = second[...]
    for p in range(SLICES):
        a1, a2, _ = spots[p]
        near[p][a2 * RING + a1] = sent[:, cuts[p]]

    wide_out[0] = twice(decay)
    wide_out[1] = twice(learned)
    wide_out[2] = twice(keys)
    high = removed.astype(BF16)
    low = (removed - high.astype(F32)).astype(BF16)
    low_out[0] = jnp.concatenate([high, low], axis=1)
    low_out[1] = jnp.concatenate([values, jnp.zeros_like(values)], axis=1).astype(BF16)

    for group in groups:
        if group != groups[0]:
            for p in group:
                onward(p, 0, mine[p])
        for offset in (1, 3, 2):
            for p in group:
                a1, a2, _ = spots[p]
                slot = near[p].at[a2 * RING + (a1 + RING - offset) % RING]
                settle(slot, r1.at[p * 3 + offset - 1])
                onward(p, offset, slot)

    for p in range(SLICES):
        a1, a2, a3 = spots[p]
        settle(near[p].at[pl.ds(0, 12)], r2.at[p])
        held = near[p][...].reshape(plane, widths[p])
        picked = dot(selectors[p % 3], held).astype(BF16)
        chosen[p][...] = picked.reshape(peers, note, widths[p])
        for offset in (1, 3, 2):
            chip = peer(strides[p][2], offset) - core
            for side in range(2):
                launch(
                    chosen[p].at[(a3 + offset) % RING * 2 + side],
                    inbox[p].at[core * RING + a3],
                    s3.at[p],
                    r3.at[p],
                    chip + side,
                )
        launch(
            chosen[p].at[a3 * 2 + 1 - core],
            inbox[p].at[core * RING + a3],
            s3.at[p],
            r3.at[p],
            partner,
        )
        inbox[p][core * RING + a3] = chosen[p][a3 * 2 + core]

    turned = (((1,), (1,)), ((), ()))
    tall_row = iota((plane, peers * note), 0)
    tall_col = iota((plane, peers * note), 1)
    expand = onehot(iota((128, peers * note), 0) == iota((128, peers * note), 1) // note)
    wanted_t = jnp.where(
        tall_row // count == tall_col % note // MOST, tall_col % MOST, -2
    ).astype(F32)

    def mixing(p):
        pick = onehot(iota((plane, every), 1) == token_of(p, iota((plane, every), 0)))
        here = lax.dot_general(pick, routes_low, turned, preferred_element_type=F32)
        weigh = lax.dot_general(pick, weights_low, turned, preferred_element_type=F32)
        number = iota((plane, 128), 1)
        names = jnp.where(number < peers, expert_of(p, number), -1).astype(F32)
        named = names < -2.0
        weight = jnp.zeros((plane, 128), F32)
        for j in range(TOPK):
            hit = here[:, j : j + 1] == names
            named = named | hit
            weight = weight + jnp.where(hit, weigh[:, j : j + 1], 0.0)
        before = dot(lower, onehot(named))
        rank = dot(jnp.where(named, before, -1.0).astype(BF16), expand)
        spread = dot(weight.astype(BF16), expand)
        return jnp.where(rank == wanted_t, spread, 0.0).astype(BF16)

    for p in range(3):
        mixers[p] = mixing(p)

    def gated(gate_part, up_part):
        return (jax.nn.silu(gate_part) * up_part).astype(BF16)

    gate_part = None
    up_part = None
    loads[2].wait()
    loads[3].wait()
    for p in range(SLICES):
        settle(inbox[p].at[pl.ds(0, 7)], r3.at[p])
        if p % 3 == 0:
            inputs = inbox[p][...].reshape(2 * each, widths[p])
        else:
            inputs = jnp.concatenate(
                [
                    dot(
                        turns[p % 3],
                        inbox[p][side * RING : (side + 1) * RING].reshape(each, widths[p]),
                    ).astype(BF16)
                    for side in range(2)
                ],
                0,
            )
        gate_more = dot(inputs, eg[cuts[p], :])
        up_more = dot(inputs, eu[cuts[p], :])
        gate_part = gate_more if gate_part is None else gate_part + gate_more
        up_part = up_more if up_part is None else up_part + up_more
    hidden = gated(gate_part, up_part)
    loads[5].wait()

    for p in range(SLICES):
        a3 = spots[p][2]
        if p % 3 == 0:
            inputs = hidden
        else:
            inputs = jnp.concatenate(
                [
                    dot(returns[p % 3], hidden[side * each : (side + 1) * each]).astype(BF16)
                    for side in range(2)
                ],
                0,
            )
        result = dot(inputs, ed[:, cuts[p]]).astype(BF16)
        answer[p][...] = result.reshape(2 * RING, note, widths[p])
        for offset in (1, 3, 2):
            chip = peer(strides[p][2], offset) - core
            for side in range(2):
                launch(
                    answer[p].at[side * RING + (a3 + offset) % RING],
                    back[p].at[a3 * 2 + core],
                    t3.at[p],
                    u3.at[p],
                    chip + side,
                )
        launch(
            answer[p].at[(1 - core) * RING + a3],
            back[p].at[a3 * 2 + core],
            t3.at[p],
            u3.at[p],
            partner,
        )
        back[p][a3 * 2 + core] = answer[p][core * RING + a3]

    loads[0].wait()
    loads[1].wait()
    shared_hidden = gated(dot(sent, sg[...]), dot(sent, su[...]))
    loads[4].wait()
    kept = after.astype(F32) + dot(shared_hidden, sd[...])

    for p in range(SLICES):
        a1, a2, a3 = spots[p]
        settle(back[p].at[pl.ds(0, 7)], u3.at[p])
        summed = dot(mixers[p % 3], back[p][...].reshape(peers * note, widths[p])).astype(BF16)
        total[p][...] = summed.reshape(RING * RING, count, widths[p])
        for offset in (1, 3, 2):
            launch(
                total[p].at[pl.ds((a2 + offset) % RING * RING, RING)],
                gather[p].at[pl.ds(offset * RING, RING)],
                t2.at[p],
                u2.at[p],
                peer(strides[p][1], offset),
            )
    for p in range(SLICES):
        a1, a2, a3 = spots[p]
        summed = total[p][pl.ds(a2 * RING, RING)].astype(F32)
        settle(gather[p].at[pl.ds(RING, 3 * RING)], u2.at[p])
        for offset in (1, 3, 2):
            summed = summed + gather[p][offset * RING : (offset + 1) * RING].astype(F32)
        line[p][...] = summed.astype(BF16)
        for offset in (1, 3, 2):
            launch(
                line[p].at[(a1 + offset) % RING],
                final[p].at[offset],
                t1.at[p],
                u1.at[p],
                peer(strides[p][0], offset),
            )
    for p in range(SLICES):
        a1 = spots[p][0]
        summed = line[p][a1].astype(F32)
        settle(final[p].at[pl.ds(1, 3)], u1.at[p])
        for offset in (1, 3, 2):
            summed = summed + final[p][offset].astype(F32)
        out[:, cuts[p]] = (kept[:, cuts[p]] + summed).astype(BF16)
    for p in range(3):
        settle(wbuf.at[p, pl.ds(0, 31)], wsend_sem.at[p])
        settle(xbuf.at[p, pl.ds(0, 7)], xsend_sem.at[p])
        settle(precv.at[p, pl.ds(0, 7)], psend_sem.at[p])
    for p in range(SLICES):
        settle(near[p].at[pl.ds(0, 15)], s1.at[p])
        settle(inbox[p].at[pl.ds(0, 7)], s3.at[p])
        settle(back[p].at[pl.ds(0, 7)], t3.at[p])
        settle(gather[p].at[pl.ds(0, 3 * RING)], t2.at[p])
        settle(final[p].at[pl.ds(0, 3)], t1.at[p])


def layer(vmems, hbms):
    tokens, routes = vmems[0], vmems[11]
    w_r, state, matrices = hbms[0], hbms[3], hbms[5:]
    count, width = tokens.shape
    rows, mix = w_r.shape
    half = mix // 2
    depth = width // RING
    heads, entries = state.shape[1:]
    widths = part_widths(width)
    vmem = pl.BlockSpec(memory_space=pltpu.VMEM)
    hbm = pl.BlockSpec(memory_space=pl.ANY)
    dma = pltpu.SemaphoreType.DMA
    blocks = RING * RING
    note = blocks * MOST
    plane = blocks * count
    shapes = (
        (RING * RING, count),
        (2 * RING, note),
        (2 * RING, note),
        (2 * RING, note),
        (2 * RING, note),
        (RING * RING, count),
        (RING * RING, count),
        (RING, count),
        (RING, count),
    )
    shapes = [pltpu.VMEM(shape + (w,), BF16) for shape in shapes for w in widths]
    sizes = [8, 3, 3 * RING, 3, 3, 3, 3]
    sizes = sizes + [SLICES * size for size in (1, 3, 1, 1, 1, 1, 1, 1, 1, 1, 1)]
    return pl.pallas_call(
        functools.partial(layer_kernel, widths),
        out_shape=[
            jax.ShapeDtypeStruct((count, width), BF16),
            jax.ShapeDtypeStruct((3, count * heads, 2 * HEAD), F32),
            jax.ShapeDtypeStruct((2, count * heads, 2 * HEAD), BF16),
        ],
        in_specs=[vmem] * len(vmems) + [hbm] * len(hbms),
        out_specs=[vmem] * 3,
        scratch_shapes=[
            pltpu.VMEM((3, 2, rows, half), BF16),
            pltpu.VMEM((3, 2 * RING * RING, rows, half), BF16),
            pltpu.VMEM((3, RING, count, depth), BF16),
            pltpu.VMEM((3, 2 * RING, count, depth), BF16),
            pltpu.VMEM((3, 2 * RING, count, half), BF16),
            pltpu.VMEM((3, 2 * RING, count, half), BF16),
            pltpu.VMEM((6, count, heads, HEAD), F32),
            pltpu.VMEM(state.shape, F32),
            pltpu.VMEM(hbms[4].shape, BF16),
        ]
        + [pltpu.VMEM(m.shape[-2:], BF16) for m in matrices]
        + [
            pltpu.VMEM((entries, HEAD), BF16),
            pltpu.VMEM((count, width), BF16),
            pltpu.VMEM((3, 2 * RING * note, plane), BF16),
            pltpu.VMEM((3, plane, 2 * RING * note), BF16),
        ]
        + shapes
        + [dma]
        + [dma((size,)) for size in sizes],
        compiler_params=pltpu.CompilerParams(
            collective_id=0, has_side_effects=True, vmem_limit_bytes=VMEM_BYTES
        ),
        name="layer",
    )(*vmems, *hbms)


def finish_kernel(wide, low, state, ready, new_state, new_tokens, spread):
    per_step, heads, entries = state.shape
    tall = per_step * heads
    span = 2 * HEAD

    @pl.when(pl.program_id(0) == 0)
    def _():
        row = lax.broadcasted_iota(jnp.int32, (span, entries), 0)
        col = lax.broadcasted_iota(jnp.int32, (span, entries), 1)
        spread[...] = onehot(col // HEAD == row % HEAD)
        new_tokens[...] = ready[...]

    decay, learned, keys = [wide[w] for w in range(3)]
    removed = dot(low[0], spread[...])
    values = dot(low[1], spread[...])
    for lane in range(0, entries, span):
        cut = slice(lane, lane + span)
        fresh = (
            state[:, :, cut].reshape(tall, span) * decay
            - removed[:, cut] * learned
            + values[:, cut] * keys
        )
        new_state[:, :, cut] = fresh.reshape(per_step, heads, span)


def finish(wide, low, state, ready):
    count, heads, entries = state.shape
    per_step = 8 if count % 8 == 0 else 1
    tall = per_step * heads
    span = 2 * HEAD
    block = pl.BlockSpec((per_step, heads, entries), lambda i: (i, 0, 0))
    flat = pl.BlockSpec(ready.shape, lambda i: (0, 0))
    return pl.pallas_call(
        finish_kernel,
        grid=(count // per_step,),
        out_shape=[
            jax.ShapeDtypeStruct(state.shape, F32),
            jax.ShapeDtypeStruct(ready.shape, BF16),
        ],
        in_specs=[
            pl.BlockSpec((3, tall, span), lambda i: (0, i, 0)),
            pl.BlockSpec((2, tall, span), lambda i: (0, i, 0)),
            block,
            flat,
        ],
        out_specs=[block, flat],
        scratch_shapes=[pltpu.VMEM((span, entries), BF16)],
        compiler_params=pltpu.CompilerParams(
            dimension_semantics=("arbitrary",), vmem_limit_bytes=VMEM_BYTES
        ),
        name="finish",
    )(wide, low, state, ready)


def per_device(
    tokens,
    recurrent_state,
    first_gain,
    w_receptance,
    w_key,
    w_value,
    decay_down,
    decay_up,
    decay_base,
    rate_down,
    rate_up,
    rate_base,
    key_scale,
    head_gain,
    w_output,
    second_gain,
    shared_gate,
    shared_up,
    shared_down,
    expert_gate,
    expert_up,
    expert_down,
    routes,
    route_weights,
):
    vmems = (
        tokens,
        first_gain[None, :],
        decay_down.T,
        decay_up,
        decay_base[None, :],
        rate_down.T,
        rate_up,
        rate_base[None, :],
        key_scale[None, :],
        head_gain[None, :],
        second_gain[None, :],
        routes.T,
        route_weights.T,
    )
    hbms = (
        w_receptance,
        w_key,
        w_value,
        recurrent_state,
        w_output,
        shared_gate,
        shared_up,
        shared_down,
        expert_gate,
        expert_up,
        expert_down,
    )
    ready, wide, low = layer(vmems, hbms)
    new_state, new_tokens = finish(wide, low, recurrent_state, ready)
    return (new_tokens, new_state)


def solution(mesh):
    in_specs = (
        P("ep", None),
        P("ep", None, None),
        P(),
        P("ep", None),
        P("ep", None),
        P("ep", None),
        P(),
        P(),
        P(),
        P(),
        P(),
        P(),
        P(),
        P(),
        P(),
        P(),
        P(),
        P(),
        P(),
        P("ep", None, None),
        P("ep", None, None),
        P("ep", None, None),
        P(),
        P(),
    )
    out_specs = (P("ep", None), P("ep", None, None))
    return jax.shard_map(
        per_device, mesh=mesh, in_specs=in_specs, out_specs=out_specs, check_vma=False
    )
```

time: 86.6 us -> 75 us (0.87)
  Pallas kernels: 84.2 us -> 74.3 us
  local copies, waits for them, and re-layouts: 1.47 us -> 0 us
    pallas_call x3 -> x2, Pallas kernels: 84.2 us -> 74.3 us  [the longest x1 69.2 us: layer(): pl.pallas_call(functools.partial(layer_kernel, widths), out_shape=[jax.Sh...]
    unnamed x1 -> x0, local copies, waits for them, and re-layouts: 1.47 us -> none
where the time goes in v4:
time: 75 us; the launch traced here: 74.9 us
  Pallas kernels  74.3 us (99%)
    pallas_call x1, Pallas kernels, layer(): pl.pallas_call(functools.partial(layer_kernel, widths), out_shape=[jax.Sh...  69.2 us
    pallas_call x1, Pallas kernels, finish(): pl.pallas_call(finish_kernel, grid=(count // per_step,), out_shape=[jax.S...  5.1 us

profile of v4, /device:TPU:1, one launch (start us, length us, event | category | flops | bytes accessed | tf_op | source)
XLA Modules:
  0.0 74.9 jit_solution(15366236283782789738)
XLA Ops:
  0.6 69.2 %layer.1 = (bf16[16,2048]{1,0:T(8,128)(2,1)}, f32[3,256,128]{2,1,0:T(8,128)}, bf16[2,256,128]{2,1,0:T(8,128)(2,1)}) custom-call(bf16[16,2048]{1,0:T(8,128)(2,1)} %tokens.1, f32[1,2048]{1,0:T(1,128)} %bitcast.14, bf16[64,2048]{1,0:T(8,128)(2,1)} %bitcast.10, bf16[64,1024]{1,0:T(8,128)(2,1)} %decay_up.1, f32[1,1024]{1,0:T(1,128)} %bitcast.16, ...), custom_call_target="tpu_custom_call" | custom-call | tf_op jit(solution)/shard_map/layer/pallas_call | solution.py:682
  69.8 5.1 %finish.1 = (f32[16,16,4096]{2,1,0:T(8,128)}, bf16[16,2048]{1,0:T(8,128)(2,1)}) custom-call(f32[3,256,128]{2,1,0:T(8,128)} %get-tuple-element.7.wide, bf16[2,256,128]{2,1,0:T(8,128)(2,1)} %get-tuple-element.8.low, f32[16,16,4096]{2,1,0:T(8,128)} %state.3, bf16[16,2048]{1,0:T(8,128)(2,1)} %get-tuple-element.9.ready), custom_call_target="tpu_custom_call" | custom-call | tf_op jit(solution)/shard_map/finish/pallas_call | solution.py:751

commit v5 on v4

--- a/solution.py
+++ b/solution.py
@@ -46,64 +46,68 @@
     return [number * 128 for number in counts]
 
 
-def layer_kernel(
-    widths,
-    tokens,
-    gain,
-    decay_down,
-    decay_up,
-    decay_base,
-    rate_down,
-    rate_up,
-    rate_base,
-    key_scale,
-    head_gain,
-    second_gain,
-    routes,
-    route_weights,
-    w_r,
-    w_k,
-    w_v,
-    state,
-    w_output,
-    shared_gate,
-    shared_up,
-    shared_down,
-    expert_gate,
-    expert_up,
-    expert_down,
-    out,
-    wide_out,
-    low_out,
-    stage,
-    wbuf,
-    nsend,
-    xbuf,
-    psend,
-    precv,
-    vecs,
-    old,
-    wo,
-    sg,
-    su,
-    sd,
-    eg,
-    eu,
-    ed,
-    fold,
-    second,
-    selectors,
-    mixers,
-    *rest,
-):
+def layer_kernel(widths, small, *refs):
+    given = refs[:small]
+    (
+        w_r,
+        w_k,
+        w_v,
+        state,
+        w_output,
+        shared_gate,
+        shared_up,
+        shared_down,
+        expert_gate,
+        expert_up,
+        expert_down,
+        out,
+        wide_out,
+        low_out,
+        stage,
+        wbuf,
+        nsend,
+        xbuf,
+        psend,
+        precv,
+        vecs,
+        old,
+        wo,
+        sg,
+        su,
+        sd,
+        eg,
+        eu,
+        ed,
+        fold,
+        second,
+        selectors,
+        mixers,
+    ) = refs[small : small + 33]
+    rest = refs[small + 33 + small :]
+    held = refs[small + 33 : small + 33 + small]
+    (
+        tokens,
+        gain,
+        decay_down,
+        decay_up,
+        decay_base,
+        rate_down,
+        rate_up,
+        rate_base,
+        key_scale,
+        head_gain,
+        second_gain,
+        routes,
+        route_weights,
+    ) = held
     near, chosen, inbox, answer, back, total, gather, line, final = [
         rest[SLICES * i : SLICES * (i + 1)] for i in range(9)
     ]
-    local_sem, load_sem = rest[9 * SLICES : 9 * SLICES + 2]
-    wsend_sem, wrecv_sem, xsend_sem, xrecv_sem, psend_sem, precv_sem = rest[
-        9 * SLICES + 2 : 9 * SLICES + 8
-    ]
-    s1, r1, r2, s3, r3, t3, u3, t2, u2, t1, u1 = rest[9 * SLICES + 8 :]
+    local_sem, load_sem, small_sem = rest[9 * SLICES : 9 * SLICES + 3]
+    wide_buf, low_buf, out_sem = rest[-3:]
+    wrecv_sem, xrecv_sem, precv_sem = rest[9 * SLICES + 3 : 9 * SLICES + 6]
+    wsend_sem, psend_sem, esend_sem, rsend_sem = rest[9 * SLICES + 6 : 9 * SLICES + 10]
+    r1, r2, r3, u3, u2, u1 = rest[9 * SLICES + 10 : -3]
     rows, mix = w_r.shape
     half = mix // 2
     count, width = tokens.shape
@@ -120,6 +124,20 @@
         return me + ((place(stride) + offset) % RING - place(stride)) * stride
 
     spots = [[place(stride) for stride in STRIDES[p % 3]] for p in range(SLICES)]
+    barrier = pltpu.get_barrier_semaphore()
+    greet = [partner]
+    for stride in STRIDES[0]:
+        for offset in range(1, RING):
+            mate = peer(stride, offset)
+            greet = greet + [mate, mate + 1 - 2 * core]
+    for mate in greet:
+        pl.semaphore_signal(barrier, inc=1, device_id=(mate,), device_id_type=MESH)
+    intake = [
+        pltpu.make_async_copy(source, target, small_sem.at[number])
+        for number, (source, target) in enumerate(zip(given, held))
+    ]
+    for copy in intake[:2]:
+        copy.start()
     local = []
     for p, weight in enumerate((w_r, w_k, w_v)):
         for side in range(2):
@@ -132,16 +150,8 @@
             )
     for copy in local:
         copy.start()
-
-    barrier = pltpu.get_barrier_semaphore()
-    greet = [partner]
-    for stride in STRIDES[0]:
-        for offset in range(1, RING):
-            mate = peer(stride, offset)
-            greet = greet + [mate, mate + 1 - 2 * core]
-    for mate in greet:
-        pl.semaphore_signal(barrier, inc=1, device_id=(mate,), device_id_type=MESH)
-
+    for copy in intake[2:]:
+        copy.start()
     loads = [
         pltpu.make_async_copy(source, target, load_sem.at[number])
         for number, (source, target) in enumerate(
@@ -157,9 +167,8 @@
             )
         )
     ]
-    for number in (6, 7, 2, 3, 5, 0, 1, 4):
-        loads[number].start()
-
+    for copy in intake[:2]:
+        copy.wait()
     normed = rms_scale(tokens[...], gain[...]).astype(BF16)
     for q in range(RING):
         nsend[0, q] = normed[:, q * depth : (q + 1) * depth]
@@ -200,14 +209,14 @@
                 launch(
                     stage.at[p, side],
                     row_slot(p, a1, a2, core),
-                    wsend_sem.at[p],
+                    wsend_sem,
                     wrecv_sem.at[p * RING + offset],
                     chip + side,
                 )
         launch(
             stage.at[p, 1 - core],
             row_slot(p, a1, a2, core),
-            wsend_sem.at[p],
+            wsend_sem,
             wrecv_sem.at[p * RING],
             partner,
         )
@@ -219,7 +228,7 @@
                 launch(
                     stage.at[p, side],
                     row_slot(p, a1, a2, core),
-                    wsend_sem.at[p],
+                    wsend_sem,
                     wrecv_sem.at[p * RING],
                     chip + side,
                 )
@@ -231,14 +240,14 @@
                 launch(
                     nsend.at[p, (a3 + offset) % RING],
                     xbuf.at[p, a3 * 2 + core],
-                    xsend_sem.at[p],
+                    wsend_sem,
                     xrecv_sem.at[p],
                     chip + side,
                 )
         launch(
             nsend.at[p, a3],
             xbuf.at[p, a3 * 2 + core],
-            xsend_sem.at[p],
+            wsend_sem,
             xrecv_sem.at[p],
             partner,
         )
@@ -247,6 +256,9 @@
         own = stage[p, core]
         wbuf[p, chip_index(p, a1, a2) * 2 + core] = own
         xbuf[p, a3 * 2 + core] = nsend[p, a3]
+
+    for number in (6, 7, 2, 3, 5, 0, 1, 4):
+        loads[number].start()
 
     for step in (1, 3, 2):
         for p in range(3):
@@ -258,10 +270,13 @@
                 launch(
                     block,
                     block,
-                    wsend_sem.at[p],
+                    wsend_sem,
                     wrecv_sem.at[p * RING],
                     peer(STRIDES[p][1], offset),
                 )
+
+    for copy in intake[2:]:
+        copy.wait()
 
     def put(number, values, first):
         for head in range(values.shape[1] // HEAD):
@@ -367,14 +382,14 @@
                 launch(
                     psend.at[p, (a3 + offset) % RING * 2 + side],
                     precv.at[p, a3 * 2 + core],
-                    psend_sem.at[p],
+                    psend_sem,
                     precv_sem.at[p],
                     chip + side,
                 )
         launch(
             psend.at[p, a3 * 2 + 1 - core],
             precv.at[p, a3 * 2 + core],
-            psend_sem.at[p],
+            psend_sem,
             precv_sem.at[p],
             partner,
         )
@@ -434,7 +449,7 @@
             launch(
                 source,
                 near[p].at[a2 * RING + (a1 + RING - step) % RING],
-                s1.at[p],
+                esend_sem,
                 r2.at[p],
                 peer(strides[p][1], offset),
             )
@@ -445,7 +460,7 @@
             launch(
                 mine[p],
                 near[p].at[a2 * RING + a1],
-                s1.at[p],
+                esend_sem,
                 r1.at[p * 3 + offset - 1],
                 peer(strides[p][0], offset),
             )
@@ -463,13 +478,19 @@
         a1, a2, _ = spots[p]
         near[p][a2 * RING + a1] = sent[:, cuts[p]]
 
-    wide_out[0] = twice(decay)
-    wide_out[1] = twice(learned)
-    wide_out[2] = twice(keys)
+    wide_buf[0] = twice(decay)
+    wide_buf[1] = twice(learned)
+    wide_buf[2] = twice(keys)
     high = removed.astype(BF16)
     low = (removed - high.astype(F32)).astype(BF16)
-    low_out[0] = jnp.concatenate([high, low], axis=1)
-    low_out[1] = jnp.concatenate([values, jnp.zeros_like(values)], axis=1).astype(BF16)
+    low_buf[0] = jnp.concatenate([high, low], axis=1)
+    low_buf[1] = jnp.concatenate([values, jnp.zeros_like(values)], axis=1).astype(BF16)
+    outward = [
+        pltpu.make_async_copy(wide_buf, wide_out, out_sem.at[0]),
+        pltpu.make_async_copy(low_buf, low_out, out_sem.at[1]),
+    ]
+    for copy in outward:
+        copy.start()
 
     for group in groups:
         if group != groups[0]:
@@ -494,14 +515,14 @@
                 launch(
                     chosen[p].at[(a3 + offset) % RING * 2 + side],
                     inbox[p].at[core * RING + a3],
-                    s3.at[p],
+                    esend_sem,
                     r3.at[p],
                     chip + side,
                 )
         launch(
             chosen[p].at[a3 * 2 + 1 - core],
             inbox[p].at[core * RING + a3],
-            s3.at[p],
+            esend_sem,
             r3.at[p],
             partner,
         )
@@ -584,14 +605,14 @@
                 launch(
                     answer[p].at[side * RING + (a3 + offset) % RING],
                     back[p].at[a3 * 2 + core],
-                    t3.at[p],
+                    rsend_sem,
                     u3.at[p],
                     chip + side,
                 )
         launch(
             answer[p].at[(1 - core) * RING + a3],
             back[p].at[a3 * 2 + core],
-            t3.at[p],
+            rsend_sem,
             u3.at[p],
             partner,
         )
@@ -612,7 +633,7 @@
             launch(
                 total[p].at[pl.ds((a2 + offset) % RING * RING, RING)],
                 gather[p].at[pl.ds(offset * RING, RING)],
-                t2.at[p],
+                rsend_sem,
                 u2.at[p],
                 peer(strides[p][1], offset),
             )
@@ -627,7 +648,7 @@
             launch(
                 line[p].at[(a1 + offset) % RING],
                 final[p].at[offset],
-                t1.at[p],
+                rsend_sem,
                 u1.at[p],
                 peer(strides[p][0], offset),
             )
@@ -638,16 +659,13 @@
         for offset in (1, 3, 2):
             summed = summed + final[p][offset].astype(F32)
         out[:, cuts[p]] = (kept[:, cuts[p]] + summed).astype(BF16)
-    for p in range(3):
-        settle(wbuf.at[p, pl.ds(0, 31)], wsend_sem.at[p])
-        settle(xbuf.at[p, pl.ds(0, 7)], xsend_sem.at[p])
-        settle(precv.at[p, pl.ds(0, 7)], psend_sem.at[p])
-    for p in range(SLICES):
-        settle(near[p].at[pl.ds(0, 15)], s1.at[p])
-        settle(inbox[p].at[pl.ds(0, 7)], s3.at[p])
-        settle(back[p].at[pl.ds(0, 7)], t3.at[p])
-        settle(gather[p].at[pl.ds(0, 3 * RING)], t2.at[p])
-        settle(final[p].at[pl.ds(0, 3)], t1.at[p])
+    sent_units = (3 * (31 + 7), 3 * 7)
+    settle(eg.at[pl.ds(0, sent_units[0] * rows)], wsend_sem)
+    settle(eg.at[pl.ds(0, sent_units[1] * rows)], psend_sem)
+    settle(wo.at[pl.ds(0, (15 + 7 * RING) * count)], esend_sem)
+    settle(wo.at[pl.ds(0, (15 + 7 * RING) * count)], rsend_sem)
+    for copy in outward:
+        copy.wait()
 
 
 def layer(vmems, hbms):
@@ -677,17 +695,17 @@
         (RING, count),
     )
     shapes = [pltpu.VMEM(shape + (w,), BF16) for shape in shapes for w in widths]
-    sizes = [8, 3, 3 * RING, 3, 3, 3, 3]
-    sizes = sizes + [SLICES * size for size in (1, 3, 1, 1, 1, 1, 1, 1, 1, 1, 1)]
+    sizes = [8, len(vmems), 3 * RING, 3, 3]
+    later = [SLICES * size for size in (3, 1, 1, 1, 1, 1)]
     return pl.pallas_call(
-        functools.partial(layer_kernel, widths),
+        functools.partial(layer_kernel, widths, len(vmems)),
         out_shape=[
             jax.ShapeDtypeStruct((count, width), BF16),
             jax.ShapeDtypeStruct((3, count * heads, 2 * HEAD), F32),
             jax.ShapeDtypeStruct((2, count * heads, 2 * HEAD), BF16),
         ],
-        in_specs=[vmem] * len(vmems) + [hbm] * len(hbms),
-        out_specs=[vmem] * 3,
+        in_specs=[hbm] * (len(vmems) + len(hbms)),
+        out_specs=[vmem, hbm, hbm],
         scratch_shapes=[
             pltpu.VMEM((3, 2, rows, half), BF16),
             pltpu.VMEM((3, 2 * RING * RING, rows, half), BF16),
@@ -706,9 +724,17 @@
             pltpu.VMEM((3, 2 * RING * note, plane), BF16),
             pltpu.VMEM((3, plane, 2 * RING * note), BF16),
         ]
+        + [pltpu.VMEM(small.shape, small.dtype) for small in vmems]
         + shapes
         + [dma]
-        + [dma((size,)) for size in sizes],
+        + [dma((size,)) for size in sizes]
+        + [dma] * 4
+        + [dma((size,)) for size in later]
+        + [
+            pltpu.VMEM((3, count * heads, 2 * HEAD), F32),
+            pltpu.VMEM((2, count * heads, 2 * HEAD), BF16),
+            dma((2,)),
+        ],
         compiler_params=pltpu.CompilerParams(
             collective_id=0, has_side_effects=True, vmem_limit_bytes=VMEM_BYTES
         ),

time: 75 us -> 73.4 us (0.979)
  Pallas kernels: 74.3 us -> 72.7 us
    pallas_call x1, Pallas kernels: 69.2 us -> 67.6 us  [layer(): pl.pallas_call(functools.partial(layer_kernel, widths, len(vmems)), out_s...]
where the time goes in v5:
time: 73.4 us; the launch traced here: 73.3 us
  Pallas kernels  72.7 us (99%)
    pallas_call x1, Pallas kernels, layer(): pl.pallas_call(functools.partial(layer_kernel, widths, len(vmems)), out_s...  67.6 us
    pallas_call x1, Pallas kernels, finish(): pl.pallas_call(finish_kernel, grid=(count // per_step,), out_shape=[jax.S...  5.1 us

profile of v5, /device:TPU:1, one launch (start us, length us, event | category | flops | bytes accessed | tf_op | source)
XLA Modules:
  0.0 73.3 jit_solution(14698545960465274157)
XLA Ops:
  0.6 67.6 %layer.1 = (bf16[16,2048]{1,0:T(8,128)(2,1)}, f32[3,256,128]{2,1,0:T(8,128)}, bf16[2,256,128]{2,1,0:T(8,128)(2,1)}) custom-call(bf16[16,2048]{1,0:T(8,128)(2,1)} %refs_0_.1, f32[1,2048]{1,0:T(1,128)} %bitcast.14, bf16[64,2048]{1,0:T(8,128)(2,1)} %bitcast.10, bf16[64,1024]{1,0:T(8,128)(2,1)} %refs_3_.1, f32[1,1024]{1,0:T(1,128)} %bitcast.16, ...), custom_call_target="tpu_custom_call" | custom-call | tf_op jit(solution)/shard_map/layer/pallas_call | solution.py:700
  68.2 5.1 %finish.1 = (f32[16,16,4096]{2,1,0:T(8,128)}, bf16[16,2048]{1,0:T(8,128)(2,1)}) custom-call(f32[3,256,128]{2,1,0:T(8,128)} %get-tuple-element.7.wide, bf16[2,256,128]{2,1,0:T(8,128)(2,1)} %get-tuple-element.8.low, f32[16,16,4096]{2,1,0:T(8,128)} %state.1, bf16[16,2048]{1,0:T(8,128)(2,1)} %get-tuple-element.9.ready), custom_call_target="tpu_custom_call" | custom-call | tf_op jit(solution)/shard_map/finish/pallas_call | solution.py:777

commit v6 on v5

--- a/solution.py
+++ b/solution.py
@@ -11,7 +11,7 @@
 TOPK = 4
 MOST = 4
 RING = 4
-SLICES = 6
+SLICES = 7
 STRIDES = ((2, 8, 32), (8, 32, 2), (32, 2, 8))
 NORM_EPS = 1e-06
 GROUP_EPS = 0.00064
@@ -42,7 +42,8 @@
 
 def part_widths(width):
     tiles = width // 128
-    counts = [tiles // SLICES + (1 if number < tiles % SLICES else 0) for number in range(SLICES)]
+    even = tiles // 3
+    counts = [even - even // 2] * 3 + [even // 2] * 3 + [tiles - 3 * even]
     return [number * 128 for number in counts]
 
 
@@ -123,7 +124,15 @@
     def peer(stride, offset):
         return me + ((place(stride) + offset) % RING - place(stride)) * stride
 
-    spots = [[place(stride) for stride in STRIDES[p % 3]] for p in range(SLICES)]
+    spots = [[place(stride) for stride in STRIDES[p % 3]] for p in range(6)]
+    spots = spots + [[spots[0][i] + core * (spots[1][i] - spots[0][i]) for i in range(3)]]
+
+    def hop(p, level, offset):
+        mate = peer(STRIDES[p % 3][level], offset)
+        return mate if p < 6 else mate + core * (peer(STRIDES[1][level], offset) - mate)
+
+    def order_of(p):
+        return p % 3 if p < 6 else core
     barrier = pltpu.get_barrier_semaphore()
     greet = [partner]
     for stride in STRIDES[0]:
@@ -451,7 +460,7 @@
                 near[p].at[a2 * RING + (a1 + RING - step) % RING],
                 esend_sem,
                 r2.at[p],
-                peer(strides[p][1], offset),
+                hop(p, 1, offset),
             )
 
     def enter(p):
@@ -462,10 +471,10 @@
                 near[p].at[a2 * RING + a1],
                 esend_sem,
                 r1.at[p * 3 + offset - 1],
-                peer(strides[p][0], offset),
+                hop(p, 0, offset),
             )
 
-    groups = [range(first, first + 3) for first in range(0, SLICES, 3)]
+    groups = [range(3), range(3, SLICES)]
     for p in groups[0]:
         enter(p)
     for p in groups[0]:
@@ -507,10 +516,10 @@
         a1, a2, a3 = spots[p]
         settle(near[p].at[pl.ds(0, 12)], r2.at[p])
         held = near[p][...].reshape(plane, widths[p])
-        picked = dot(selectors[p % 3], held).astype(BF16)
+        picked = dot(selectors[order_of(p)], held).astype(BF16)
         chosen[p][...] = picked.reshape(peers, note, widths[p])
         for offset in (1, 3, 2):
-            chip = peer(strides[p][2], offset) - core
+            chip = hop(p, 2, offset) - core
             for side in range(2):
                 launch(
                     chosen[p].at[(a3 + offset) % RING * 2 + side],
@@ -559,25 +568,28 @@
     def gated(gate_part, up_part):
         return (jax.nn.silu(gate_part) * up_part).astype(BF16)
 
+    def turned_by(matrices, p, side, inputs):
+        which = p % 3 if p < 6 else side
+        return inputs if which == 0 else dot(matrices[which], inputs).astype(BF16)
+
     gate_part = None
     up_part = None
     loads[2].wait()
     loads[3].wait()
     for p in range(SLICES):
         settle(inbox[p].at[pl.ds(0, 7)], r3.at[p])
-        if p % 3 == 0:
-            inputs = inbox[p][...].reshape(2 * each, widths[p])
-        else:
-            inputs = jnp.concatenate(
-                [
-                    dot(
-                        turns[p % 3],
-                        inbox[p][side * RING : (side + 1) * RING].reshape(each, widths[p]),
-                    ).astype(BF16)
-                    for side in range(2)
-                ],
-                0,
-            )
+        inputs = jnp.concatenate(
+            [
+                turned_by(
+                    turns,
+                    p,
+                    side,
+                    inbox[p][side * RING : (side + 1) * RING].reshape(each, widths[p]),
+                )
+                for side in range(2)
+            ],
+            0,
+        )
         gate_more = dot(inputs, eg[cuts[p], :])
         up_more = dot(inputs, eu[cuts[p], :])
         gate_part = gate_more if gate_part is None else gate_part + gate_more
@@ -587,36 +599,36 @@
 
     for p in range(SLICES):
         a3 = spots[p][2]
-        if p % 3 == 0:
-            inputs = hidden
-        else:
-            inputs = jnp.concatenate(
-                [
-                    dot(returns[p % 3], hidden[side * each : (side + 1) * each]).astype(BF16)
-                    for side in range(2)
-                ],
-                0,
-            )
+        inputs = jnp.concatenate(
+            [
+                turned_by(returns, p, side, hidden[side * each : (side + 1) * each])
+                for side in range(2)
+            ],
+            0,
+        )
         result = dot(inputs, ed[:, cuts[p]]).astype(BF16)
         answer[p][...] = result.reshape(2 * RING, note, widths[p])
-        for offset in (1, 3, 2):
-            chip = peer(strides[p][2], offset) - core
+        ends = [spots[p][2] if p < 6 else spots[side][2] for side in range(2)]
+        for offset in (1, 3, 2):
             for side in range(2):
+                stride = STRIDES[p % 3 if p < 6 else side][2]
                 launch(
-                    answer[p].at[side * RING + (a3 + offset) % RING],
-                    back[p].at[a3 * 2 + core],
+                    answer[p].at[side * RING + (ends[side] + offset) % RING],
+                    back[p].at[ends[side] * 2 + core],
                     rsend_sem,
                     u3.at[p],
-                    chip + side,
+                    peer(stride, offset) - core + side,
                 )
+        end = ends[0] + core * (ends[1] - ends[0])
+        far = ends[0] + ends[1] - end
         launch(
-            answer[p].at[(1 - core) * RING + a3],
-            back[p].at[a3 * 2 + core],
+            answer[p].at[(1 - core) * RING + far],
+            back[p].at[far * 2 + core],
             rsend_sem,
             u3.at[p],
             partner,
         )
-        back[p][a3 * 2 + core] = answer[p][core * RING + a3]
+        back[p][end * 2 + core] = answer[p][core * RING + end]
 
     loads[0].wait()
     loads[1].wait()
@@ -627,7 +639,7 @@
     for p in range(SLICES):
         a1, a2, a3 = spots[p]
         settle(back[p].at[pl.ds(0, 7)], u3.at[p])
-        summed = dot(mixers[p % 3], back[p][...].reshape(peers * note, widths[p])).astype(BF16)
+        summed = dot(mixers[order_of(p)], back[p][...].reshape(peers * note, widths[p])).astype(BF16)
         total[p][...] = summed.reshape(RING * RING, count, widths[p])
         for offset in (1, 3, 2):
             launch(
@@ -635,7 +647,7 @@
                 gather[p].at[pl.ds(offset * RING, RING)],
                 rsend_sem,
                 u2.at[p],
-                peer(strides[p][1], offset),
+                hop(p, 1, offset),
             )
     for p in range(SLICES):
         a1, a2, a3 = spots[p]
@@ -650,7 +662,7 @@
                 final[p].at[offset],
                 rsend_sem,
                 u1.at[p],
-                peer(strides[p][0], offset),
+                hop(p, 0, offset),
             )
     for p in range(SLICES):
         a1 = spots[p][0]

time: 73.4 us -> 72.2 us (0.984)
  Pallas kernels: 72.7 us -> 71.4 us
    pallas_call x1, Pallas kernels: 67.6 us -> 66.3 us  [layer(): pl.pallas_call(functools.partial(layer_kernel, widths, len(vmems)), out_s...]
where the time goes in v6:
time: 72.2 us; the launch traced here: 72 us
  Pallas kernels  71.4 us (99%)
    pallas_call x1, Pallas kernels, layer(): pl.pallas_call(functools.partial(layer_kernel, widths, len(vmems)), out_s...  66.3 us
    pallas_call x1, Pallas kernels, finish(): pl.pallas_call(finish_kernel, grid=(count // per_step,), out_shape=[jax.S...  5.09 us

profile of v6, /device:TPU:1, one launch (start us, length us, event | category | flops | bytes accessed | tf_op | source)
XLA Modules:
  0.0 72.0 jit_solution(8009624421304979195)
XLA Ops:
  0.6 66.3 %layer.1 = (bf16[16,2048]{1,0:T(8,128)(2,1)}, f32[3,256,128]{2,1,0:T(8,128)}, bf16[2,256,128]{2,1,0:T(8,128)(2,1)}) custom-call(bf16[16,2048]{1,0:T(8,128)(2,1)} %refs_0_.1, f32[1,2048]{1,0:T(1,128)} %bitcast.14, bf16[64,2048]{1,0:T(8,128)(2,1)} %bitcast.10, bf16[64,1024]{1,0:T(8,128)(2,1)} %refs_3_.1, f32[1,1024]{1,0:T(1,128)} %bitcast.16, ...), custom_call_target="tpu_custom_call" | custom-call | tf_op jit(solution)/shard_map/layer/pallas_call | solution.py:712
  66.9 5.1 %finish.1 = (f32[16,16,4096]{2,1,0:T(8,128)}, bf16[16,2048]{1,0:T(8,128)(2,1)}) custom-call(f32[3,256,128]{2,1,0:T(8,128)} %get-tuple-element.7.wide, bf16[2,256,128]{2,1,0:T(8,128)(2,1)} %get-tuple-element.8.low, f32[16,16,4096]{2,1,0:T(8,128)} %state.1, bf16[16,2048]{1,0:T(8,128)(2,1)} %get-tuple-element.9.ready), custom_call_target="tpu_custom_call" | custom-call | tf_op jit(solution)/shard_map/finish/pallas_call | solution.py:789

commit v7 on v6

--- a/solution.py
+++ b/solution.py
@@ -212,7 +212,7 @@
 
     for p in range(3):
         a1, a2, _ = spots[p]
-        for offset in (1, 3, 2):
+        for offset in (2, 1, 3):
             chip = peer(STRIDES[p][0], offset) - core
             for side in range(2):
                 launch(
@@ -231,7 +231,7 @@
         )
     for p in range(3):
         a1, a2, _ = spots[p]
-        for offset in (1, 3, 2):
+        for offset in (2, 1, 3):
             chip = peer(STRIDES[p][1], offset) - core
             for side in range(2):
                 launch(
@@ -243,7 +243,7 @@
                 )
     for p in range(3):
         a3 = spots[p][2]
-        for offset in (1, 3, 2):
+        for offset in (2, 1, 3):
             chip = peer(STRIDES[p][2], offset) - core
             for side in range(2):
                 launch(
@@ -275,7 +275,7 @@
             first = (a1 + RING - step) % RING
             block = wbuf.at[p, pl.ds(chip_index(p, first, a2) * 2, 2)]
             settle(block, wrecv_sem.at[p * RING + step])
-            for offset in (1, 3, 2):
+            for offset in (2, 1, 3):
                 launch(
                     block,
                     block,
@@ -385,7 +385,7 @@
         stacked = xbuf[p].reshape(2 * RING * count, depth)
         part = dot(stacked, wbuf[p].reshape(depth, half)).astype(BF16)
         psend[p] = part.reshape(2 * RING, count, half)
-        for offset in (1, 3, 2):
+        for offset in (2, 1, 3):
             chip = peer(STRIDES[p][2], offset) - core
             for side in range(2):
                 launch(
@@ -454,7 +454,7 @@
 
     def onward(p, step, source):
         a1, a2, _ = spots[p]
-        for offset in (1, 3, 2):
+        for offset in (2, 1, 3):
             launch(
                 source,
                 near[p].at[a2 * RING + (a1 + RING - step) % RING],
@@ -465,7 +465,7 @@
 
     def enter(p):
         a1, a2, _ = spots[p]
-        for offset in (1, 3, 2):
+        for offset in (2, 1, 3):
             launch(
                 mine[p],
                 near[p].at[a2 * RING + a1],
@@ -518,7 +518,7 @@
         held = near[p][...].reshape(plane, widths[p])
         picked = dot(selectors[order_of(p)], held).astype(BF16)
         chosen[p][...] = picked.reshape(peers, note, widths[p])
-        for offset in (1, 3, 2):
+        for offset in (2, 1, 3):
             chip = hop(p, 2, offset) - core
             for side in range(2):
                 launch(
@@ -609,7 +609,7 @@
         result = dot(inputs, ed[:, cuts[p]]).astype(BF16)
         answer[p][...] = result.reshape(2 * RING, note, widths[p])
         ends = [spots[p][2] if p < 6 else spots[side][2] for side in range(2)]
-        for offset in (1, 3, 2):
+        for offset in (2, 1, 3):
             for side in range(2):
                 stride = STRIDES[p % 3 if p < 6 else side][2]
                 launch(
@@ -641,7 +641,7 @@
         settle(back[p].at[pl.ds(0, 7)], u3.at[p])
         summed = dot(mixers[order_of(p)], back[p][...].reshape(peers * note, widths[p])).astype(BF16)
         total[p][...] = summed.reshape(RING * RING, count, widths[p])
-        for offset in (1, 3, 2):
+        for offset in (2, 1, 3):
             launch(
                 total[p].at[pl.ds((a2 + offset) % RING * RING, RING)],
                 gather[p].at[pl.ds(offset * RING, RING)],
@@ -656,7 +656,7 @@
         for offset in (1, 3, 2):
             summed = summed + gather[p][offset * RING : (offset + 1) * RING].astype(F32)
         line[p][...] = summed.astype(BF16)
-        for offset in (1, 3, 2):
+        for offset in (2, 1, 3):
             launch(
                 line[p].at[(a1 + offset) % RING],
                 final[p].at[offset],

time: 72.2 us -> 71 us (0.983)
  Pallas kernels: 71.4 us -> 70.2 us
    pallas_call x1, Pallas kernels: 66.3 us -> 65.1 us  [layer(): pl.pallas_call(functools.partial(layer_kernel, widths, len(vmems)), out_s...]
where the time goes in v7:
time: 71 us; the launch traced here: 70.8 us
  Pallas kernels  70.2 us (99%)
    pallas_call x1, Pallas kernels, layer(): pl.pallas_call(functools.partial(layer_kernel, widths, len(vmems)), out_s...  65.1 us
    pallas_call x1, Pallas kernels, finish(): pl.pallas_call(finish_kernel, grid=(count // per_step,), out_shape=[jax.S...  5.09 us

profile of v7, /device:TPU:1, one launch (start us, length us, event | category | flops | bytes accessed | tf_op | source)
XLA Modules:
  0.0 70.8 jit_solution(11256833887377293164)
XLA Ops:
  0.6 65.1 %layer.1 = (bf16[16,2048]{1,0:T(8,128)(2,1)}, f32[3,256,128]{2,1,0:T(8,128)}, bf16[2,256,128]{2,1,0:T(8,128)(2,1)}) custom-call(bf16[16,2048]{1,0:T(8,128)(2,1)} %refs_0_.1, f32[1,2048]{1,0:T(1,128)} %bitcast.14, bf16[64,2048]{1,0:T(8,128)(2,1)} %bitcast.10, bf16[64,1024]{1,0:T(8,128)(2,1)} %refs_3_.1, f32[1,1024]{1,0:T(1,128)} %bitcast.16, ...), custom_call_target="tpu_custom_call" | custom-call | tf_op jit(solution)/shard_map/layer/pallas_call | solution.py:712
  65.7 5.1 %finish.1 = (f32[16,16,4096]{2,1,0:T(8,128)}, bf16[16,2048]{1,0:T(8,128)(2,1)}) custom-call(f32[3,256,128]{2,1,0:T(8,128)} %get-tuple-element.7.wide, bf16[2,256,128]{2,1,0:T(8,128)(2,1)} %get-tuple-element.8.low, f32[16,16,4096]{2,1,0:T(8,128)} %state.1, bf16[16,2048]{1,0:T(8,128)(2,1)} %get-tuple-element.9.ready), custom_call_target="tpu_custom_call" | custom-call | tf_op jit(solution)/shard_map/finish/pallas_call | solution.py:789
